TPU v7x, 512 devices: a whole 4x4x16 slice. The times are simulated.
512 devices in a mesh: ep: 32 (over z, core), tp: 16 (over y, x).
Axes of the slice: x: 4, y: 4, z: 16, core: 2. Of those that a mesh axis runs over, the one named last changes fastest.
Arguments:
- hidden: bfloat16 [384, 2048], P('ep'), may hold values from -6 to 6
- pre_gain: bfloat16 [2048], replicated, may hold values from 0.099609375 to 1.8984375
- query_weight: bfloat16 [2048, 1024], P('ep', 'tp'), may hold values from -0.125 to 0.125
- key_cache: bfloat16 [384, 1024, 1024], P('ep', 'tp'), may hold values from -6 to 6
- value_cache: bfloat16 [384, 1024, 1024], P('ep', 'tp'), may hold values from -6 to 6
- lengths: int32 [384], P('ep'), may hold values from 128 to 1024
- stick_bias: float32 [16], P('tp'), may hold values from -8.5 to -3
- out_weight: bfloat16 [1024, 2048], P('tp', 'ep'), may hold values from -0.1875 to 0.1875
- post_gain: bfloat16 [2048], replicated, may hold values from 0.099609375 to 1.8984375
- ffn_gain: bfloat16 [2048], replicated, may hold values from 0.099609375 to 1.8984375
- expert_ids: int32 [384, 2], P('ep'), may hold values from 0 to 31, as said below
- route_logits: float32 [384, 2], P('ep'), may hold values from -6 to 6
- gate_experts: bfloat16 [32, 2048, 2048], P('ep', None, 'tp'), may hold values from -0.125 to 0.125
- up_experts: bfloat16 [32, 2048, 2048], P('ep', None, 'tp'), may hold values from -0.125 to 0.125
- down_experts: bfloat16 [32, 2048, 2048], P('ep', 'tp'), may hold values from -2 to 2
- out_gain: bfloat16 [2048], P('tp'), may hold values from 0.099609375 to 1.8984375
Outputs:
- result: bfloat16 [384, 2048], P('ep', 'tp')
Inputs may be any that keep to these rules, and one draw needn't show every extreme that they name: `expert_ids`: each row names 2 different experts of one group of 4 consecutive experts. Among the rows of one device (aligned blocks of 12 rows) no expert is named more than 2 times, and one expert is named exactly 2 times in every block.
All inputs are finite; a program needn't handle non-finite values.
Results may differ from a plain program's by a relative error of at most 0.014.
Values may be sent and summed in bfloat16 or wider, within the bound.
A program may use at most 64 MiB of HBM per device.

v0:
```python
import jax
import jax.numpy as jnp
from jax import lax
from jax.sharding import PartitionSpec as P

epsilon = 1e-06


def copy_for_each(value, axis):
    length = lax.axis_size(axis)
    return lax.all_to_all(
        jnp.broadcast_to(value[None], (length, *value.shape)), axis, 0, 0, tiled=True
    )


def laid_out(blocks, dim):
    dims = list(blocks.shape[1:])
    dims[dim] *= blocks.shape[0]
    return jnp.moveaxis(blocks, 0, dim).reshape(dims)


def gather_directly(value, axis, dim):
    blocks = copy_for_each(value, axis)
    return laid_out(blocks, dim)


def taken_together(value, axis):
    return copy_for_each(value, axis).sum(axis=0)


def cut_along(value, dim, length):
    dims = value.shape
    blocks = value.reshape(*dims[:dim], length, dims[dim] // length, *dims[dim + 1 :])
    return jnp.moveaxis(blocks, dim, 0)


def summed_on_arrival(value, axis, dim):
    length = lax.axis_size(axis)
    blocks = lax.all_to_all(cut_along(value, dim, length), axis, 0, 0, tiled=True)
    return jnp.sum(blocks, axis=0)


def inverse_rms(squares, features):
    return lax.rsqrt(squares / features + epsilon)


def stick_read(queries, key_blocks, value_blocks, lengths, head_bias):
    sequences, heads, head_size = queries.shape
    positions = key_blocks.shape[3]
    scores = jnp.einsum("she,shec->shc", queries, key_blocks, preferred_element_type=jnp.float32)
    scores = scores * head_size ** (-0.5) + head_bias[None, :, None]
    places = lax.broadcasted_iota(jnp.int32, (sequences, heads, positions), 2)
    inside = places < lengths[:, None, None]
    log_fail = jnp.where(inside, jax.nn.log_sigmoid(-scores), 0.0)
    after_sum = lax.cumsum(log_fail, axis=2, reverse=True) - log_fail
    weight = jnp.where(inside, jnp.exp(jax.nn.log_sigmoid(scores) + after_sum), 0.0).astype(
        jnp.bfloat16
    )
    mixed_heads = jnp.einsum(
        "shc,shec->she", weight, value_blocks, preferred_element_type=jnp.float32
    )
    return mixed_heads.astype(jnp.bfloat16)


def per_device(
    hidden,
    pre_gain,
    query_weight,
    key_cache,
    value_cache,
    lengths,
    stick_bias,
    out_weight,
    post_gain,
    ffn_gain,
    expert_ids,
    route_logits,
    gate_experts,
    up_experts,
    down_experts,
    out_gain,
):
    sequences, features = hidden.shape
    ep_count = lax.axis_size("ep")
    tp_count = lax.axis_size("tp")
    tp_place = lax.axis_index("tp")
    heads_here = stick_bias.shape[0]
    head_size = key_cache.shape[1] // heads_here
    positions = key_cache.shape[2]
    slice_width = features // tp_count
    hidden_wide = hidden.astype(jnp.float32)
    normed = (
        hidden_wide
        * inverse_rms(jnp.sum(hidden_wide * hidden_wide, axis=1, keepdims=True), features)
        * pre_gain.astype(jnp.float32)
    ).astype(jnp.bfloat16)
    queries = jnp.dot(
        normed, gather_directly(query_weight, "ep", 0), preferred_element_type=jnp.float32
    )
    queries = queries.astype(jnp.bfloat16).reshape(sequences, heads_here, head_size)
    key_blocks = key_cache.reshape(sequences, heads_here, head_size, positions)
    value_blocks = value_cache.reshape(sequences, heads_here, head_size, positions)
    mixed_heads = stick_read(queries, key_blocks, value_blocks, lengths, stick_bias)
    mixed_heads = mixed_heads.reshape(sequences, heads_here * head_size)
    partial_value = jnp.dot(
        mixed_heads, gather_directly(out_weight, "ep", 1), preferred_element_type=jnp.float32
    )
    attended = taken_together(partial_value, "tp").astype(jnp.bfloat16)
    attended = lax.optimization_barrier(attended).astype(jnp.float32)
    residual = (
        hidden_wide
        + attended
        * inverse_rms(jnp.sum(attended * attended, axis=1, keepdims=True), features)
        * post_gain.astype(jnp.float32)
    ).astype(jnp.bfloat16)
    residual_wide = residual.astype(jnp.float32)
    ffn_in = (
        residual_wide
        * inverse_rms(jnp.sum(residual_wide * residual_wide, axis=1, keepdims=True), features)
        * ffn_gain.astype(jnp.float32)
    ).astype(jnp.bfloat16)
    pick_count = expert_ids.shape[1]
    local_experts = gate_experts.shape[0]
    experts_total = local_experts * ep_count
    capacity = max(2, (2 * pick_count * sequences + experts_total - 1) // experts_total)
    flat_ids = expert_ids.reshape(-1)
    choose = (flat_ids[:, None] == lax.broadcasted_iota(jnp.int32, (1, experts_total), 1)).astype(
        jnp.int32
    )
    earlier = jnp.cumsum(choose, axis=0) - choose
    slot_of = jnp.sum(earlier * choose, axis=1)
    target = (flat_ids * capacity + slot_of).reshape(sequences, pick_count)
    slot_iota = lax.broadcasted_iota(jnp.int32, (experts_total * capacity, 1, 1), 0)
    placing = jnp.any(slot_iota == target[None, :, :], axis=2).astype(jnp.bfloat16)
    outgoing = jnp.dot(placing, ffn_in, preferred_element_type=jnp.float32).astype(jnp.bfloat16)
    outgoing = outgoing.reshape(ep_count, local_experts, capacity, features)
    arrived = lax.all_to_all(outgoing, "ep", split_axis=0, concat_axis=0, tiled=True)
    gate_act = jnp.einsum(
        "nlcd,ldf->nlcf", arrived, gate_experts, preferred_element_type=jnp.float32
    )
    up_act = jnp.einsum("nlcd,ldf->nlcf", arrived, up_experts, preferred_element_type=jnp.float32)
    active = (jax.nn.silu(gate_act) * up_act).astype(jnp.bfloat16)
    partial_out = jnp.einsum(
        "nlcf,lfd->nlcd", active, down_experts, preferred_element_type=jnp.float32
    )
    summed = summed_on_arrival(partial_out, "tp", 3).astype(jnp.bfloat16)
    returned = lax.all_to_all(summed, "ep", split_axis=0, concat_axis=0, tiled=True)
    result_table = returned.reshape(experts_total * capacity, slice_width)
    selector = (
        target.reshape(-1)[:, None]
        == lax.broadcasted_iota(jnp.int32, (1, experts_total * capacity), 1)
    ).astype(jnp.bfloat16)
    picked = jnp.dot(selector, result_table, preferred_element_type=jnp.float32)
    picked = picked.reshape(sequences, pick_count, slice_width)
    route_weight = jax.nn.softmax(route_logits, axis=1)
    combined = jnp.sum(route_weight[:, :, None] * picked, axis=1)
    squares = taken_together(jnp.sum(combined * combined, axis=1), "tp")
    own_residual = lax.dynamic_slice_in_dim(residual_wide, tp_place * slice_width, slice_width, 1)
    result = own_residual + combined * inverse_rms(squares, features)[:, None] * out_gain.astype(
        jnp.float32
    )
    return result.astype(jnp.bfloat16)


def solution(mesh):
    placed = (
        P("ep", None),
        P(),
        P("ep", "tp"),
        P("ep", "tp", None),
        P("ep", "tp", None),
        P("ep"),
        P("tp"),
        P("tp", "ep"),
        P(),
        P(),
        P("ep", None),
        P("ep", None),
        P("ep", None, "tp"),
        P("ep", None, "tp"),
        P("ep", "tp", None),
        P("tp"),
    )
    return jax.shard_map(
        per_device, mesh=mesh, in_specs=placed, out_specs=P("ep", "tp"), check_vma=False
    )
```

profile of v0, /device:TPU:1, one launch (start us, length us, event | category | flops | bytes accessed | tf_op | source)
XLA Modules:
  0.0 189.8 jit_solution(8275066417072983527)
XLA Ops:
  0.0 0.9 broadcast_in_dim.11
  1.0 1.1 reshape.225
  2.1 16.7 %all-to-all-start = ((bf16[32,2,2048]{2,1,0:T(2,128)(2,1)}), bf16[32,2,2048]{2,1,0:T(2,128)(2,1)S(1)}, u32[]{:S(2)}, u32[]{:S(2)}) async-start(bf16[32,2,2048]{2,1,0:T(2,128)(2,1)} %reshape.225), calls=%async_computation | async-start | bytes 524288 | tf_op jit(solution)/shard_map/all_to_all | solution.py:11
  19.6 1.1 reshape.223
  20.9 20.2 %all-to-all-done = bf16[32,2,2048]{2,1,0:T(2,128)(2,1)S(1)} async-done(((bf16[32,2,2048]{2,1,0:T(2,128)(2,1)}), bf16[32,2,2048]{2,1,0:T(2,128)(2,1)S(1)}, u32[]{:S(2)}, u32[]{:S(2)}) %all-to-all-start) | async-done | bytes 262176 | tf_op jit(solution)/shard_map/all_to_all | solution.py:11
  41.1 4.2 %all-to-all-start.1 = ((bf16[32,2,2048]{2,1,0:T(2,128)(2,1)}), bf16[32,2,2048]{2,1,0:T(2,128)(2,1)S(1)}, u32[]{:S(2)}, u32[]{:S(2)}) async-start(bf16[32,2,2048]{2,1,0:T(2,128)(2,1)} %reshape.223), calls=%async_computation.1 | async-start | bytes 524288 | tf_op jit(solution)/shard_map/all_to_all | solution.py:11
  45.3 0.4 reshape.226
  45.9 0.3 fusion.49
  46.3 14.9 %reduce-window.6 = f32[12,1,8,128]{3,2,1,0:T(8,128)S(1)} reduce-window(f32[12,1,8,128]{3,2,1,0:T(8,128)S(1)} %slice_bitcast_fusion, f32[]{:T(128)} %constant.13.clone.1), window={size=1x1x1x128 pad=0_0x0_0x0_0x0_127}, to_apply=%region_1.2 | reduce-window | flops 1560576 | bytes 98308 | tf_op jit(solution)/shard_map/reduce-window
  61.6 5.3 %all-to-all-done.1 = bf16[32,2,2048]{2,1,0:T(2,128)(2,1)S(1)} async-done(((bf16[32,2,2048]{2,1,0:T(2,128)(2,1)}), bf16[32,2,2048]{2,1,0:T(2,128)(2,1)S(1)}, u32[]{:S(2)}, u32[]{:S(2)}) %all-to-all-start.1) | async-done | bytes 262176 | tf_op jit(solution)/shard_map/all_to_all | solution.py:11
  66.9 0.4 reshape.224
  67.3 0.3 copy.88
  67.6 0.5 reshape.206
  68.2 1.9 %fusion.35 = bf16[12,1,64]{2,1,0:T(2,128)(2,1)S(1)} fusion(bf16[12,64,1024]{2,1,0:T(8,128)(2,1)} %param.20, bf16[12,1024,1]{1,0,2:T(8,128)(2,1)S(1)} %fusion.42), kind=kOutput, calls=%fused_computation.50 | convolution fusion | flops 1572864 | bytes 1598976 | tf_op jit(solution)/shard_map/shc,shec->she/dot_general | solution.py:59
  70.3 1.5 broadcast_in_dim.13
  71.8 6.9 %all-to-all-start.2 = ((f32[16,12,2048]{2,1,0:T(8,128)}), f32[16,12,2048]{2,1,0:T(8,128)}, u32[]{:S(2)}, u32[]{:S(2)}) async-start(f32[16,12,2048]{2,1,0:T(8,128)} %broadcast_in_dim.13), calls=%async_computation.2 | async-start | bytes 4194304 | tf_op jit(solution)/shard_map/all_to_all | solution.py:11
  79.6 27.4 %all-to-all-done.2 = f32[16,12,2048]{2,1,0:T(8,128)} async-done(((f32[16,12,2048]{2,1,0:T(8,128)}), f32[16,12,2048]{2,1,0:T(8,128)}, u32[]{:S(2)}, u32[]{:S(2)}) %all-to-all-start.2) | async-done | bytes 1572896 | tf_op jit(solution)/shard_map/all_to_all | solution.py:11
  107.0 1.7 reduce_sum.93
  109.1 0.3 convolution_convert_fusion
  109.6 34.0 %all_to_all.36 = bf16[32,1,2,2048]{3,2,1,0:T(2,128)(2,1)S(1)} all-to-all(bf16[32,1,2,2048]{3,2,1,0:T(2,128)(2,1)S(1)} %bitcast.114), channel_id=1, replica_groups=mesh['ep'=32,'tp'=16] {'ep'}, dimensions={0} | all-to-all | bytes 524288 | tf_op jit(solution)/shard_map/all_to_all | solution.py:137
  143.6 0.2 convolution_bitcast_fusion.2
  143.9 1.5 convolution_bitcast_fusion
  145.3 0.9 copy.134
  146.2 3.6 %all-to-all-start.4 = ((f32[16,32,1,2,128]{4,1,3,2,0:T(8,128)}), f32[16,32,1,2,128]{4,1,3,2,0:T(8,128)S(1)}, u32[]{:S(2)}, u32[]{:S(2)}) async-start(f32[16,32,1,2,128]{4,1,3,2,0:T(8,128)} %bitcast.108), calls=%async_computation.4 | async-start | bytes 1048576 | tf_op jit(solution)/shard_map/all_to_all | solution.py:39
  149.8 10.5 %all-to-all-done.4 = f32[16,32,1,2,128]{4,1,3,2,0:T(8,128)S(1)} async-done(((f32[16,32,1,2,128]{4,1,3,2,0:T(8,128)}), f32[16,32,1,2,128]{4,1,3,2,0:T(8,128)S(1)}, u32[]{:S(2)}, u32[]{:S(2)}) %all-to-all-start.4) | async-done | bytes 524320 | tf_op jit(solution)/shard_map/all_to_all | solution.py:39
  160.4 0.6 copy.96
  161.0 5.4 %all-to-all-start.5 = ((bf16[32,1,2,128]{3,2,1,0:T(2,128)(2,1)}), bf16[32,1,2,128]{3,2,1,0:T(2,128)(2,1)S(1)}, u32[]{:S(2)}, u32[]{:S(2)}) async-start(bf16[32,1,2,128]{3,2,1,0:T(2,128)(2,1)} %copy.96), calls=%async_computation.5 | async-start | bytes 32768 | tf_op jit(solution)/shard_map/all_to_all | solution.py:147
  166.4 11.9 %all-to-all-done.5 = bf16[32,1,2,128]{3,2,1,0:T(2,128)(2,1)S(1)} async-done(((bf16[32,1,2,128]{3,2,1,0:T(2,128)(2,1)}), bf16[32,1,2,128]{3,2,1,0:T(2,128)(2,1)S(1)}, u32[]{:S(2)}, u32[]{:S(2)}) %all-to-all-start.5) | async-done | bytes 16416 | tf_op jit(solution)/shard_map/all_to_all | solution.py:147
  178.6 0.6 broadcast_in_dim.14
  179.2 3.5 %all-to-all-start.6 = ((f32[16,1,12]{2,1,0:T(1,128)}), f32[16,1,12]{2,1,0:T(1,128)S(1)}, u32[]{:S(2)}, u32[]{:S(2)}) async-start(f32[16,1,12]{2,1,0:T(1,128)} %broadcast_in_dim.14), calls=%async_computation.6 | async-start | bytes 16384 | tf_op jit(solution)/shard_map/all_to_all | solution.py:11
  182.7 6.3 %all-to-all-done.6 = f32[16,1,12]{2,1,0:T(1,128)S(1)} async-done(((f32[16,1,12]{2,1,0:T(1,128)}), f32[16,1,12]{2,1,0:T(1,128)S(1)}, u32[]{:S(2)}, u32[]{:S(2)}) %all-to-all-start.6) | async-done | bytes 800 | tf_op jit(solution)/shard_map/all_to_all | solution.py:11
  189.1 0.7 add_convert_fusion
  (68 shorter events, 3.0 us)
Async XLA Ops:
  0.0 45.9 %copy-start = (bf16[12,64,1024]{2,1,0:T(8,128)(2,1)S(1)}, bf16[12,64,1024]{2,1,0:T(8,128)(2,1)}, u32[]{:S(2)}) copy-start(bf16[12,64,1024]{2,1,0:T(8,128)(2,1)} %param.19) | copy-start | bytes 4718596
  0.0 18.8 %copy-start.6 = (bf16[2048]{0:T(1024)(128)(2,1)S(1)}, bf16[2048]{0:T(1024)(128)(2,1)}, u32[]{:S(2)}) copy-start(bf16[2048]{0:T(1024)(128)(2,1)} %param.17) | copy-start | bytes 12292
  0.0 19.5 %copy-start.4 = (bf16[64,64]{1,0:T(8,128)(2,1)S(1)}, bf16[64,64]{1,0:T(8,128)(2,1)}, u32[]{:S(2)}) copy-start(bf16[64,64]{1,0:T(8,128)(2,1)} %param.23) | copy-start | bytes 24580
  0.0 20.7 %copy-start.1 = (bf16[12,2048]{1,0:T(8,128)(2,1)S(1)}, bf16[12,2048]{1,0:T(8,128)(2,1)}, u32[]{:S(2)}) copy-start(bf16[12,2048]{1,0:T(8,128)(2,1)} %param.16) | copy-start | bytes 147460
  2.1 39.0 %all-to-all-start = ((bf16[32,2,2048]{2,1,0:T(2,128)(2,1)}), bf16[32,2,2048]{2,1,0:T(2,128)(2,1)S(1)}, u32[]{:S(2)}, u32[]{:S(2)}) async-start(bf16[32,2,2048]{2,1,0:T(2,128)(2,1)} %reshape.225), calls=%async_computation | async-start | bytes 524288 | tf_op jit(solution)/shard_map/all_to_all | solution.py:11
  41.1 25.8 %all-to-all-start.1 = ((bf16[32,2,2048]{2,1,0:T(2,128)(2,1)}), bf16[32,2,2048]{2,1,0:T(2,128)(2,1)S(1)}, u32[]{:S(2)}, u32[]{:S(2)}) async-start(bf16[32,2,2048]{2,1,0:T(2,128)(2,1)} %reshape.223), calls=%async_computation.1 | async-start | bytes 524288 | tf_op jit(solution)/shard_map/all_to_all | solution.py:11
  45.3 0.9 copy-start.10
  71.8 7.0 %copy-start.7 = (bf16[2048]{0:T(1024)(128)(2,1)S(1)}, bf16[2048]{0:T(1024)(128)(2,1)}, u32[]{:S(2)}) copy-start(bf16[2048]{0:T(1024)(128)(2,1)} %param.24) | copy-start | bytes 12292
  71.8 7.0 %copy-start.9 = (s32[12,2]{0,1:T(2,128)S(1)}, s32[12,2]{0,1:T(2,128)}, u32[]{:S(2)}) copy-start(s32[12,2]{0,1:T(2,128)} %param.26) | copy-start | bytes 292
  71.8 7.6 %copy-start.8 = (bf16[2048]{0:T(1024)(128)(2,1)S(1)}, bf16[2048]{0:T(1024)(128)(2,1)}, u32[]{:S(2)}) copy-start(bf16[2048]{0:T(1024)(128)(2,1)} %param.25) | copy-start | bytes 12292
  71.8 35.2 %all-to-all-start.2 = ((f32[16,12,2048]{2,1,0:T(8,128)}), f32[16,12,2048]{2,1,0:T(8,128)}, u32[]{:S(2)}, u32[]{:S(2)}) async-start(f32[16,12,2048]{2,1,0:T(8,128)} %broadcast_in_dim.13), calls=%async_computation.2 | async-start | bytes 4194304 | tf_op jit(solution)/shard_map/all_to_all | solution.py:11
  79.6 64.0 %copy-start.3 = (bf16[1,2048,128]{2,1,0:T(8,128)(2,1)S(1)}, bf16[1,2048,128]{2,1,0:T(8,128)(2,1)}, u32[]{:S(2)}) copy-start(bf16[1,2048,128]{2,1,0:T(8,128)(2,1)} %param.28) | copy-start | bytes 1572868
  108.7 35.1 %copy-start.2 = (bf16[1,128,2048]{2,1,0:T(8,128)(2,1)S(1)}, bf16[1,128,2048]{2,1,0:T(8,128)(2,1)}, u32[]{:S(2)}) copy-start(bf16[1,128,2048]{2,1,0:T(8,128)(2,1)} %param.30) | copy-start | bytes 1572868
  143.9 5.9 %copy-start.5 = (f32[12,2]{0,1:T(2,128)S(1)}, f32[12,2]{0,1:T(2,128)}, u32[]{:S(2)}) copy-start(f32[12,2]{0,1:T(2,128)} %param.27) | copy-start | bytes 292
  145.3 37.4 %copy-start.11 = (bf16[128]{0:T(256)(128)(2,1)S(1)}, bf16[128]{0:T(256)(128)(2,1)}, u32[]{:S(2)}) copy-start(bf16[128]{0:T(256)(128)(2,1)} %param.31) | copy-start | bytes 772
  146.2 14.2 %all-to-all-start.4 = ((f32[16,32,1,2,128]{4,1,3,2,0:T(8,128)}), f32[16,32,1,2,128]{4,1,3,2,0:T(8,128)S(1)}, u32[]{:S(2)}, u32[]{:S(2)}) async-start(f32[16,32,1,2,128]{4,1,3,2,0:T(8,128)} %bitcast.108), calls=%async_computation.4 | async-start | bytes 1048576 | tf_op jit(solution)/shard_map/all_to_all | solution.py:39
  161.0 17.3 %all-to-all-start.5 = ((bf16[32,1,2,128]{3,2,1,0:T(2,128)(2,1)}), bf16[32,1,2,128]{3,2,1,0:T(2,128)(2,1)S(1)}, u32[]{:S(2)}, u32[]{:S(2)}) async-start(bf16[32,1,2,128]{3,2,1,0:T(2,128)(2,1)} %copy.96), calls=%async_computation.5 | async-start | bytes 32768 | tf_op jit(solution)/shard_map/all_to_all | solution.py:147
  179.2 9.9 %all-to-all-start.6 = ((f32[16,1,12]{2,1,0:T(1,128)}), f32[16,1,12]{2,1,0:T(1,128)S(1)}, u32[]{:S(2)}, u32[]{:S(2)}) async-start(f32[16,1,12]{2,1,0:T(1,128)} %broadcast_in_dim.14), calls=%async_computation.6 | async-start | bytes 16384 | tf_op jit(solution)/shard_map/all_to_all | solution.py:11
where the time goes:
time: 190 us
  waiting for transfers between devices  81.7 us (43%)
  starting transfers between devices  40.3 us (21%)
  blocking collectives  34 us (18%)
  other arithmetic  18.6 us (10%)
  local copies, waits for them, and re-layouts  9.33 us (5%)
  matrix products  4.82 us (3%)
    all_to_all x4, waiting for transfers between devices, copy_for_each(): lax.all_to_all(jnp.broadcast_to(value[None], (length, *value.shape)), axi...  59.3 us
    all_to_all x1, blocking collectives, per_device(): lax.all_to_all(outgoing, 'ep', split_axis=0, concat_axis=0, tiled=True)  34 us
    all_to_all x4, starting transfers between devices, copy_for_each(): lax.all_to_all(jnp.broadcast_to(value[None], (length, *value.shape)), axi...  31.3 us
    another operation x2, other arithmetic  14.9 us
    all_to_all x1, waiting for transfers between devices, per_device(): lax.all_to_all(summed, 'ep', split_axis=0, concat_axis=0, tiled=True)  11.9 us
    all_to_all x1, waiting for transfers between devices, summed_on_arrival(): lax.all_to_all(cut_along(value, dim, length), axis, 0, 0, tiled=True)  10.5 us
    all_to_all x1, starting transfers between devices, per_device(): lax.all_to_all(summed, 'ep', split_axis=0, concat_axis=0, tiled=True)  5.36 us
  transfers between devices with their start and end apart: 6, of which 6 were waited for; matrix products, arithmetic and copies ran while one was open for 10% of the time, Pallas kernels for 0%

commit v1 on v0

v1 whole, which is shorter than its diff:
```python
import functools

import jax
import jax.numpy as jnp
from jax import lax
from jax.experimental import pallas as pl
from jax.experimental.pallas import tpu as pltpu
from jax.sharding import PartitionSpec as P

epsilon = 1e-06
F32 = jnp.float32
BF16 = jnp.bfloat16
MESH = pl.DeviceIdType.MESH
NT = (((1,), (1,)), ((), ()))


def iota(shape, dim):
    return lax.broadcasted_iota(jnp.int32, shape, dim)


def inverse_rms(squares, features):
    return lax.rsqrt(squares / features + epsilon)


def eye(n):
    return (iota((n, n), 0) == iota((n, n), 1)).astype(BF16)


def transposed(value):
    return lax.dot_general(
        eye(value.shape[1]), value.astype(BF16), NT, preferred_element_type=F32
    )


def three_parts(value):
    high = value.astype(BF16)
    rest = value - high.astype(F32)
    middle = rest.astype(BF16)
    low = (rest - middle.astype(F32)).astype(BF16)
    return high, middle, low


def layer_kernel(
    ep_count,
    tp_count,
    hidden_ref,
    pre_gain_ref,
    query_weight_ref,
    key_hbm,
    value_hbm,
    lengths_ref,
    stick_bias_ref,
    out_weight_ref,
    post_gain_ref,
    ffn_gain_ref,
    expert_ids_ref,
    route_logits_ref,
    gate_hbm,
    up_hbm,
    down_hbm,
    out_gain_ref,
    result_ref,
    keys,
    values,
    gates,
    ups,
    downs,
    wq_all,
    wo_all,
    wo_full,
    scores_scr,
    stick_scr,
    place_scr,
    mix_scr,
    ids_scr,
    logits_scr,
    own_scr,
    gain_scr,
    tri_scr,
    rs_out,
    rs_in,
    hz_out,
    hz_in,
    az_out,
    az_in,
    h_rows,
    a_rows,
    r_scr,
    f_scr,
    ex_out,
    ex_in,
    back_out,
    back_in,
    asq_in,
    csq_in,
    load_sem,
    wq_recv,
    wo_recv,
    recv_sem,
    send_sem,
):
    me = lax.axis_index("ep")
    mine = lax.axis_index("tp")
    place = me // 2
    core = lax.rem(me, 2)
    partner = me + 1 - 2 * core
    chips = ep_count // 2
    half = chips // 2
    sequences, features = hidden_ref.shape
    padded = 16
    positions = keys.shape[2]
    head_size = keys.shape[1]
    width = features // tp_count
    blocks = positions // 128

    barrier = pltpu.get_barrier_semaphore()

    def greet_ep(d, carry):
        pl.semaphore_signal(
            barrier, inc=1, device_id=(lax.rem(me + d, ep_count), mine), device_id_type=MESH
        )
        return carry

    def greet_tp(d, carry):
        pl.semaphore_signal(
            barrier, inc=1, device_id=(me, lax.rem(mine + d, tp_count)), device_id_type=MESH
        )
        return carry

    lax.fori_loop(1, ep_count, greet_ep, 0)
    lax.fori_loop(1, tp_count, greet_tp, 0)

    loads = [
        pltpu.make_async_copy(key_hbm, keys, load_sem.at[0]),
        pltpu.make_async_copy(value_hbm, values, load_sem.at[1]),
        pltpu.make_async_copy(gate_hbm.at[0], gates, load_sem.at[2]),
        pltpu.make_async_copy(up_hbm.at[0], ups, load_sem.at[3]),
        pltpu.make_async_copy(down_hbm.at[0], downs, load_sem.at[4]),
    ]
    for load in loads:
        load.start()

    wq = query_weight_ref[...].astype(F32)
    rows_half = wq.shape[0] // 2
    wq_all[me, 0] = jnp.concatenate([wq[:rows_half], wq[rows_half:]], axis=1).astype(BF16)
    wo = out_weight_ref[...].astype(F32)
    wo_half = wo.shape[0] // 2
    wo_all[me] = jnp.concatenate([wo[:wo_half], wo[wo_half:]], axis=1).astype(BF16)

    hidden = hidden_ref[...].astype(F32)
    normed = (
        hidden
        * inverse_rms(jnp.sum(hidden * hidden, axis=1, keepdims=True), features)
        * pre_gain_ref[...].astype(F32).reshape(1, features)
    ).astype(BF16)

    own_columns = pl.ds(pl.multiple_of(mine * width, width), width)
    own_scr[...] = jnp.zeros_like(own_scr)
    own_scr[0:sequences, :] = hidden_ref[:, own_columns].astype(F32)
    ids_scr[...] = jnp.full(ids_scr.shape, -1, jnp.int32)
    ids_scr[0:sequences, :] = expert_ids_ref[...]
    logits_scr[...] = jnp.zeros_like(logits_scr)
    logits_scr[0:sequences, :] = route_logits_ref[...]
    scores_scr[...] = jnp.zeros_like(scores_scr)
    post_gain = post_gain_ref[...].astype(F32).reshape(1, features)
    for c in range(tp_count):
        gain_scr[c] = post_gain[:, width * c : width * c + width]

    ids = ids_scr[...]
    lanes = iota((padded, ep_count), 1)
    picks = [(ids[:, k : k + 1] == lanes).astype(F32) for k in range(2)]
    either = picks[0] + picks[1]
    before = (iota((padded, padded), 1) < iota((padded, padded), 0)).astype(BF16)
    earlier = jnp.dot(before, either.astype(BF16), preferred_element_type=F32)
    logits = logits_scr[...]
    first, second = logits[:, 0:1], logits[:, 1:2]
    top = jnp.maximum(first, second)
    first, second = jnp.exp(first - top), jnp.exp(second - top)
    weighted = picks[0] * (first / (first + second)) + picks[1] * (second / (first + second))
    for s in range(2):
        at_slot = (earlier == float(s)).astype(F32)
        place_scr[s] = transposed(either * at_slot)
        mix_scr[s] = weighted * at_slot

    for s in range(2):
        hz_out[:, s, :] = jnp.dot(
            place_scr[s].astype(BF16), own_scr[...].astype(BF16), preferred_element_type=F32
        )

    tri_scr[:, 0:128] = (iota((128, 128), 0) > iota((128, 128), 1)).astype(BF16)
    tri_scr[:, 128:256] = jnp.ones((128, 128), BF16)

    row_of = iota((padded, 128), 0)
    length_of = jnp.zeros((padded, 128), jnp.int32)
    for b in range(sequences):
        length_of = jnp.where(row_of == b, lengths_ref[b], length_of)

    pl.semaphore_wait(barrier, ep_count + tp_count - 2)

    def far_first(step):
        odd = lax.rem(step, 2)
        off = half + (1 - odd) * (step // 2) - odd * ((step + 1) // 2)
        return lax.rem(place + off, chips)

    def wq_copy(owner, target, sem, slot):
        return pltpu.make_async_remote_copy(
            src_ref=wq_all.at[owner, 0],
            dst_ref=wq_all.at[owner, 0],
            send_sem=send_sem.at[slot],
            recv_sem=sem,
            device_id=(target, mine),
            device_id_type=MESH,
        )

    def wo_copy(owner, target, sem, slot):
        return pltpu.make_async_remote_copy(
            src_ref=wo_all.at[owner],
            dst_ref=wo_all.at[owner],
            send_sem=send_sem.at[slot],
            recv_sem=sem,
            device_id=(target, mine),
            device_id_type=MESH,
        )

    def send_along(copy, recv, slot):
        def step(s, carry):
            copy(me, 2 * far_first(s) + core, recv.at[place], slot).start()
            return carry

        lax.fori_loop(0, chips - 1, step, 0)

    def z_exchange(source, target_ref, sem_at):
        def step(s, carry):
            to = 2 * far_first(s // 2) + lax.rem(s, 2)
            pltpu.make_async_remote_copy(
                src_ref=source.at[to],
                dst_ref=target_ref.at[me],
                send_sem=send_sem.at[sem_at],
                recv_sem=recv_sem.at[sem_at],
                device_id=(to, mine),
                device_id_type=MESH,
            ).start()
            return carry

        lax.fori_loop(0, 2 * (chips - 1), step, 0)
        pltpu.make_async_remote_copy(
            src_ref=source.at[partner],
            dst_ref=target_ref.at[me],
            send_sem=send_sem.at[sem_at],
            recv_sem=recv_sem.at[sem_at],
            device_id=(partner, mine),
            device_id_type=MESH,
        ).start()

    def tp_exchange(source, target_ref, sem_at, scatter):
        def step(d, carry):
            to = lax.rem(mine + d, tp_count)
            pltpu.make_async_remote_copy(
                src_ref=source.at[to] if scatter else source.at[mine],
                dst_ref=target_ref.at[mine],
                send_sem=send_sem.at[sem_at],
                recv_sem=recv_sem.at[sem_at],
                device_id=(me, to),
                device_id_type=MESH,
            ).start()
            return carry

        lax.fori_loop(1, tp_count, step, 0)

    def bytes_of(ref, count, sem):
        some = ref.at[pl.ds(0, count)]
        pltpu.make_async_copy(some, some, sem).wait()

    WQ_RELAY, WO_RELAY, HZ, HR, RS, ASQ, AZ, AR, EX, BACK, CSQ = range(11)
    WQ_SEND, WO_SEND = 11, 12

    send_along(wq_copy, wq_recv, WQ_SEND)
    wq_copy(me, partner, recv_sem.at[WQ_RELAY], WQ_RELAY).start()
    send_along(wo_copy, wo_recv, WO_SEND)
    wo_copy(me, partner, recv_sem.at[WO_RELAY], WO_RELAY).start()
    z_exchange(hz_out, hz_in, HZ)

    def relay(copy, recv, slot):
        def step(d, carry):
            off = (d + 1) // 2
            odd = lax.rem(d, 2)
            source = lax.rem(place + odd * off + (1 - odd) * (chips - off), chips)
            owner = 2 * source + core
            copy(owner, partner, recv.at[source], slot).wait_recv()
            copy(owner, partner, recv_sem.at[slot], slot).start()
            return carry

        lax.fori_loop(1, chips, step, 0)

    relay(wq_copy, wq_recv, WQ_RELAY)
    bytes_of(wq_all.at[:, 0], chips, recv_sem.at[WQ_RELAY])

    for i in range(ep_count):
        wq_all[i, 1] = pltpu.roll(wq_all[i, 0].astype(F32), 64, 1).astype(BF16)
    queries = jnp.dot(
        normed, wq_all[...].reshape(features, 128), preferred_element_type=F32
    )[:, 0:head_size]
    query_columns = transposed(queries)

    loads[0].wait()
    for b in range(sequences):
        product = keys[b].astype(F32) * query_columns[:, b : b + 1]
        scores_scr[b : b + 1, :] = jnp.sum(product, axis=0, keepdims=True)
    bias = stick_bias_ref[0]
    fails, log_hits, insides = [], [], []
    for c in range(blocks):
        score = scores_scr[:, 128 * c : 128 * c + 128] * head_size ** (-0.5) + bias
        inside = iota((padded, 128), 1) + 128 * c < length_of
        soft = jnp.log1p(jnp.exp(-jnp.abs(score)))
        log_hits.append(jnp.minimum(score, 0.0) - soft)
        fails.append(jnp.where(inside, jnp.minimum(-score, 0.0) - soft, 0.0))
        insides.append(inside)
    stacked = jnp.concatenate(fails, axis=0)
    sums = jnp.dot(
        jnp.concatenate(three_parts(stacked), axis=0), tri_scr[...], preferred_element_type=F32
    )
    count = padded * blocks
    sums = (sums[2 * count :] + sums[count : 2 * count]) + sums[:count]
    later = jnp.zeros((padded, 128), F32)
    for c in reversed(range(blocks)):
        block = sums[padded * c : padded * c + padded]
        after = block[:, 0:128] + later
        stick_scr[:, 128 * c : 128 * c + 128] = jnp.where(
            insides[c], jnp.exp(log_hits[c] + after), 0.0
        ).astype(BF16)
        later = later + block[:, 128:256]

    loads[1].wait()
    read = lax.dot_general(
        values[...].reshape(sequences * head_size, positions),
        stick_scr[...],
        NT,
        preferred_element_type=F32,
    )
    column = iota((head_size, padded), 1)
    mixed_columns = jnp.zeros((head_size, padded), F32)
    for b in range(sequences):
        mixed_columns = jnp.where(
            column == b, read[head_size * b : head_size * b + head_size], mixed_columns
        )
    mixed = transposed(mixed_columns).astype(BF16)

    relay(wo_copy, wo_recv, WO_RELAY)
    bytes_of(wo_all, chips, recv_sem.at[WO_RELAY])
    left = iota((wo_half, 128), 1) < 64
    for c in range(chips):
        one, two = wo_all[2 * c].astype(F32), wo_all[2 * c + 1].astype(F32)
        columns = slice(128 * c, 128 * c + 128)
        wo_full[0:wo_half, columns] = jnp.where(left, one, pltpu.roll(two, 64, 1)).astype(BF16)
        wo_full[wo_half : 2 * wo_half, columns] = jnp.where(
            left, pltpu.roll(one, 64, 1), two
        ).astype(BF16)
    for c in range(tp_count):
        rs_out[c] = jnp.dot(
            mixed, wo_full[:, width * c : width * c + width], preferred_element_type=F32
        ).astype(BF16)
    tp_exchange(rs_out, rs_in, RS, True)
    rs_in[mine] = rs_out[mine]

    bytes_of(hz_in, ep_count - 1, recv_sem.at[HZ])
    hz_in[me] = hz_out[me]
    h_rows[mine] = jnp.concatenate([hz_in[:, 0, :], hz_in[:, 1, :]], axis=0).astype(BF16)
    tp_exchange(h_rows, h_rows, HR, False)

    bytes_of(rs_in, tp_count - 1, recv_sem.at[RS])
    total = rs_in[0].astype(F32)
    for c in range(1, tp_count):
        total = total + rs_in[c].astype(F32)
    attended = total.astype(BF16)

    for s in range(2):
        az_out[:, s, :] = jnp.dot(
            place_scr[s].astype(BF16), attended, preferred_element_type=F32
        )
    z_exchange(az_out, az_in, AZ)
    az_in[me] = az_out[me]

    diagonal = iota((padded, 128), 0) == iota((padded, 128), 1)

    def as_row(value):
        return jnp.sum(
            jnp.where(diagonal, jnp.sum(value * value, axis=1, keepdims=True), 0.0),
            axis=0,
            keepdims=True,
        )

    def as_column(row):
        return jnp.sum(jnp.where(diagonal, row, 0.0), axis=1, keepdims=True)

    attended = attended.astype(F32)
    asq_in[mine] = as_row(attended)
    tp_exchange(asq_in, asq_in, ASQ, False)
    bytes_of(h_rows, tp_count - 1, recv_sem.at[HR])

    bytes_of(az_in, ep_count - 1, recv_sem.at[AZ])
    a_rows[mine] = jnp.concatenate([az_in[:, 0, :], az_in[:, 1, :]], axis=0).astype(BF16)
    tp_exchange(a_rows, a_rows, AR, False)

    bytes_of(asq_in, tp_count - 1, recv_sem.at[ASQ])
    squares = as_column(jnp.sum(asq_in[:, 0, :], axis=0, keepdims=True))
    own_gain = gain_scr[mine]
    own_scr[...] = (
        (own_scr[...] + attended * inverse_rms(squares, features) * own_gain)
        .astype(BF16)
        .astype(F32)
    )
    for load in loads[2:]:
        load.wait()

    bytes_of(a_rows, tp_count - 1, recv_sem.at[AR])
    rows = 2 * ep_count
    post_gain = post_gain_ref[...].astype(F32).reshape(1, features)
    ffn_gain = ffn_gain_ref[...].astype(F32).reshape(1, features)
    square = jnp.zeros((rows, width), F32)
    for c in range(tp_count):
        one = a_rows[c].astype(F32)
        square = square + one * one
    scale = inverse_rms(jnp.sum(square, axis=1, keepdims=True), features)
    square = jnp.zeros((rows, width), F32)
    for c in range(tp_count):
        columns = slice(width * c, width * c + width)
        one = (
            h_rows[c].astype(F32) + a_rows[c].astype(F32) * scale * post_gain[:, columns]
        ).astype(BF16)
        r_scr[c] = one
        one = one.astype(F32)
        square = square + one * one
    scale = inverse_rms(jnp.sum(square, axis=1, keepdims=True), features)
    for c in range(tp_count):
        columns = slice(width * c, width * c + width)
        f_scr[:, columns] = (r_scr[c].astype(F32) * scale * ffn_gain[:, columns]).astype(BF16)
    ffn_in = f_scr[...]
    gate_act = jnp.dot(ffn_in, gates[...], preferred_element_type=F32)
    up_act = jnp.dot(ffn_in, ups[...], preferred_element_type=F32)
    active = (gate_act / (1.0 + jnp.exp(-gate_act)) * up_act).astype(BF16)
    for c in range(tp_count):
        ex_out[c] = jnp.dot(
            active, downs[:, width * c : width * c + width], preferred_element_type=F32
        ).astype(BF16)
    tp_exchange(ex_out, ex_in, EX, True)
    ex_in[mine] = ex_out[mine]
    bytes_of(ex_in, tp_count - 1, recv_sem.at[EX])
    total = ex_in[0].astype(F32)
    for c in range(1, tp_count):
        total = total + ex_in[c].astype(F32)
    total = total.astype(BF16).astype(F32)

    for s in range(2):
        back_out[:, s, :] = total[ep_count * s : ep_count * s + ep_count]
    z_exchange(back_out, back_in, BACK)
    back_in[me] = back_out[me]
    bytes_of(back_in, ep_count - 1, recv_sem.at[BACK])
    combined = jnp.zeros((padded, width), F32)
    for s in range(2):
        table = back_in[:, s, :].astype(BF16)
        for part in reversed(three_parts(mix_scr[s])):
            combined = combined + jnp.dot(part, table, preferred_element_type=F32)

    csq_in[mine] = as_row(combined)
    tp_exchange(csq_in, csq_in, CSQ, False)

    bytes_of(wq_all.at[:, 0], chips - 1, send_sem.at[WQ_SEND])
    bytes_of(wq_all.at[:, 0], chips, send_sem.at[WQ_RELAY])
    bytes_of(wo_all, chips - 1, send_sem.at[WO_SEND])
    bytes_of(wo_all, chips, send_sem.at[WO_RELAY])
    for ref, slot in ((hz_out, HZ), (az_out, AZ), (back_out, BACK)):
        bytes_of(ref, ep_count - 1, send_sem.at[slot])
    for ref, slot in (
        (rs_out, RS),
        (h_rows, HR),
        (asq_in, ASQ),
        (a_rows, AR),
        (ex_out, EX),
    ):
        bytes_of(ref, tp_count - 1, send_sem.at[slot])

    bytes_of(csq_in, tp_count - 1, recv_sem.at[CSQ])
    squares = as_column(jnp.sum(csq_in[:, 0, :], axis=0, keepdims=True))
    out_gain = out_gain_ref[...].astype(F32).reshape(1, width)
    result = own_scr[...] + combined * inverse_rms(squares, features) * out_gain
    result_ref[...] = result[0:sequences].astype(BF16)
    bytes_of(csq_in, tp_count - 1, send_sem.at[CSQ])


def per_device(
    hidden,
    pre_gain,
    query_weight,
    key_cache,
    value_cache,
    lengths,
    stick_bias,
    out_weight,
    post_gain,
    ffn_gain,
    expert_ids,
    route_logits,
    gate_experts,
    up_experts,
    down_experts,
    out_gain,
):
    ep_count = lax.axis_size("ep")
    tp_count = lax.axis_size("tp")
    sequences, features = hidden.shape
    positions = key_cache.shape[2]
    width = features // tp_count
    chips = ep_count // 2
    rows = 2 * ep_count
    vmem = pl.BlockSpec(memory_space=pltpu.VMEM)
    smem = pl.BlockSpec(memory_space=pltpu.SMEM)
    hbm = pl.BlockSpec(memory_space=pl.ANY)
    scratch = [
        pltpu.VMEM(key_cache.shape, BF16),
        pltpu.VMEM(value_cache.shape, BF16),
        pltpu.VMEM(gate_experts.shape[1:], BF16),
        pltpu.VMEM(up_experts.shape[1:], BF16),
        pltpu.VMEM(down_experts.shape[1:], BF16),
        pltpu.VMEM((ep_count, 2, 32, 128), BF16),
        pltpu.VMEM((ep_count, 32, 128), BF16),
        pltpu.VMEM((64, features), BF16),
        pltpu.VMEM((16, positions), F32),
        pltpu.VMEM((16, positions), BF16),
        pltpu.VMEM((2, ep_count, 16), F32),
        pltpu.VMEM((2, 16, ep_count), F32),
        pltpu.VMEM((16, 2), jnp.int32),
        pltpu.VMEM((16, 2), F32),
        pltpu.VMEM((16, width), F32),
        pltpu.VMEM((tp_count, 1, width), F32),
        pltpu.VMEM((128, 256), BF16),
        pltpu.VMEM((tp_count, 16, width), BF16),
        pltpu.VMEM((tp_count, 16, width), BF16),
        pltpu.VMEM((ep_count, 2, width), F32),
        pltpu.VMEM((ep_count, 2, width), F32),
        pltpu.VMEM((ep_count, 2, width), F32),
        pltpu.VMEM((ep_count, 2, width), F32),
        pltpu.VMEM((tp_count, rows, width), BF16),
        pltpu.VMEM((tp_count, rows, width), BF16),
        pltpu.VMEM((tp_count, rows, width), BF16),
        pltpu.VMEM((rows, features), BF16),
        pltpu.VMEM((tp_count, rows, width), BF16),
        pltpu.VMEM((tp_count, rows, width), BF16),
        pltpu.VMEM((ep_count, 2, width), F32),
        pltpu.VMEM((ep_count, 2, width), F32),
        pltpu.VMEM((tp_count, 1, width), F32),
        pltpu.VMEM((tp_count, 1, width), F32),
        pltpu.SemaphoreType.DMA((5,)),
        pltpu.SemaphoreType.DMA((chips,)),
        pltpu.SemaphoreType.DMA((chips,)),
        pltpu.SemaphoreType.DMA((13,)),
        pltpu.SemaphoreType.DMA((13,)),
    ]
    return pl.pallas_call(
        functools.partial(layer_kernel, ep_count, tp_count),
        out_shape=jax.ShapeDtypeStruct((sequences, width), BF16),
        in_specs=[
            vmem,
            vmem,
            vmem,
            hbm,
            hbm,
            smem,
            smem,
            vmem,
            vmem,
            vmem,
            vmem,
            vmem,
            hbm,
            hbm,
            hbm,
            vmem,
        ],
        out_specs=vmem,
        scratch_shapes=scratch,
        compiler_params=pltpu.CompilerParams(collective_id=0, has_side_effects=True),
        name="layer",
    )(
        hidden,
        pre_gain,
        query_weight,
        key_cache,
        value_cache,
        lengths,
        stick_bias,
        out_weight,
        post_gain,
        ffn_gain,
        expert_ids,
        route_logits,
        gate_experts,
        up_experts,
        down_experts,
        out_gain,
    )


def solution(mesh):
    placed = (
        P("ep", None),
        P(),
        P("ep", "tp"),
        P("ep", "tp", None),
        P("ep", "tp", None),
        P("ep"),
        P("tp"),
        P("tp", "ep"),
        P(),
        P(),
        P("ep", None),
        P("ep", None),
        P("ep", None, "tp"),
        P("ep", None, "tp"),
        P("ep", "tp", None),
        P("tp"),
    )
    return jax.shard_map(
        per_device, mesh=mesh, in_specs=placed, out_specs=P("ep", "tp"), check_vma=False
    )
```

time: 190 us -> 75.7 us (0.40)
  waiting for transfers between devices: 81.7 us -> 0 us
  Pallas kernels: 0 us -> 70.8 us
  starting transfers between devices: 40.3 us -> 0 us
  blocking collectives: 34 us -> 0 us
  other arithmetic: 18.6 us -> 0 us
  local copies, waits for them, and re-layouts: 9.33 us -> 3.97 us
  matrix products: 4.82 us -> 0 us
    all_to_all x6 -> x0, waiting for transfers between devices: 81.7 us -> none  [the longest x4 59.3 us: copy_for_each(): lax.all_to_all(jnp.broadcast_to(value[None], (length, *value.shape)), axi...]
    pallas_call x0 -> x1, Pallas kernels: none -> 70.8 us  [per_device(): pl.pallas_call(functools.partial(layer_kernel, ep_count, tp_count), out_s...]
    all_to_all x6 -> x0, starting transfers between devices: 40.3 us -> none  [the longest x4 31.3 us: copy_for_each(): lax.all_to_all(jnp.broadcast_to(value[None], (length, *value.shape)), axi...]
    all_to_all x1 -> x0, blocking collectives: 34 us -> none  [per_device(): lax.all_to_all(outgoing, 'ep', split_axis=0, concat_axis=0, tiled=True)]
    another operation x3 -> x0, other arithmetic: 14.9 us -> none
    dot_general x8 -> x0, matrix products: 4.82 us -> none  [the longest x1 1.92 us: stick_read(): jnp.einsum('shc,shec->she', weight, value_blocks, preferred_element_type=...]
    broadcast_in_dim x4 -> x0, local copies, waits for them, and re-layouts: 3.21 us -> none  [copy_for_each(): jnp.broadcast_to(value[None], (length, *value.shape))]
    reduce_sum x9 -> x0, other arithmetic: 2.58 us -> none  [the longest x2 1.74 us: taken_together(): return copy_for_each(value, axis).sum(axis=0)]
  transfers between devices with their start and end apart: 6 -> 0, of which waited for: 6 -> 0; matrix products, arithmetic and copies ran while one was open for 10% -> 0% of each run, Pallas kernels for 0% -> 0%
where the time goes in v1:
time: 75.7 us; the launch traced here: 75.4 us
  Pallas kernels  70.8 us (94%)
  local copies, waits for them, and re-layouts  3.97 us (5%)
    pallas_call x1, Pallas kernels, per_device(): pl.pallas_call(functools.partial(layer_kernel, ep_count, tp_count), out_s...  70.8 us
    unnamed x3, local copies, waits for them, and re-layouts  3.97 us

profile of v1, /device:TPU:1, one launch (start us, length us, event | category | flops | bytes accessed | tf_op | source)
XLA Modules:
  0.0 75.4 jit_solution(4721124530919553024)
XLA Ops:
  0.7 1.4 %copy.17.expert_ids_ref = s32[12,2]{1,0:T(8,128)} copy(s32[12,2]{0,1:T(2,128)} %param.26) | data formatting | bytes 192 | tf_op args[10]
  2.0 1.3 %copy.18.route_logits_ref = f32[12,2]{1,0:T(8,128)} copy(f32[12,2]{0,1:T(2,128)} %param.27) | data formatting | bytes 192 | tf_op args[11]
  3.4 70.8 %layer.1 = bf16[12,128]{1,0:T(8,128)(2,1)} custom-call(bf16[12,2048]{1,0:T(8,128)(2,1)} %hidden_ref.1, bf16[2048]{0:T(1024)(128)(2,1)} %pre_gain_ref.1, bf16[64,64]{1,0:T(8,128)(2,1)} %query_weight_ref.1, bf16[12,64,1024]{2,1,0:T(8,128)(2,1)} %key_hbm.1, bf16[12,64,1024]{2,1,0:T(8,128)(2,1)} %value_hbm.1, s32[12]{0:T(128)} %lengths_ref.1, ...), custom_call_target="tpu_custom_call" | custom-call | tf_op jit(solution)/shard_map/layer/pallas_call | solution.py:558
  74.2 1.3 %copy.21 = bf16[12,128]{1,0:T(8,128)(2,1)} copy(bf16[12,128]{1,0:T(8,128)(2,1)} %layer.1) | data formatting | bytes 6144

commit v2 on v1

--- a/solution.py
+++ b/solution.py
@@ -43,11 +43,26 @@
 def layer_kernel(
     ep_count,
     tp_count,
+    hidden_hbm,
+    pre_gain_hbm,
+    query_weight_hbm,
+    key_hbm,
+    value_hbm,
+    lengths_hbm,
+    stick_bias_hbm,
+    out_weight_hbm,
+    post_gain_hbm,
+    ffn_gain_hbm,
+    expert_ids_hbm,
+    route_logits_hbm,
+    gate_hbm,
+    up_hbm,
+    down_hbm,
+    out_gain_hbm,
+    result_ref,
     hidden_ref,
     pre_gain_ref,
     query_weight_ref,
-    key_hbm,
-    value_hbm,
     lengths_ref,
     stick_bias_ref,
     out_weight_ref,
@@ -55,11 +70,7 @@
     ffn_gain_ref,
     expert_ids_ref,
     route_logits_ref,
-    gate_hbm,
-    up_hbm,
-    down_hbm,
     out_gain_ref,
-    result_ref,
     keys,
     values,
     gates,
@@ -72,8 +83,6 @@
     stick_scr,
     place_scr,
     mix_scr,
-    ids_scr,
-    logits_scr,
     own_scr,
     gain_scr,
     tri_scr,
@@ -94,6 +103,7 @@
     asq_in,
     csq_in,
     load_sem,
+    small_sem,
     wq_recv,
     wo_recv,
     recv_sem,
@@ -106,6 +116,7 @@
     partner = me + 1 - 2 * core
     chips = ep_count // 2
     half = chips // 2
+    reach = chips // 4
     sequences, features = hidden_ref.shape
     padded = 16
     positions = keys.shape[2]
@@ -115,21 +126,40 @@
 
     barrier = pltpu.get_barrier_semaphore()
 
-    def greet_ep(d, carry):
-        pl.semaphore_signal(
-            barrier, inc=1, device_id=(lax.rem(me + d, ep_count), mine), device_id_type=MESH
+    def greet(target):
+        pl.semaphore_signal(barrier, inc=1, device_id=target, device_id_type=MESH)
+
+    def chip_at(off):
+        return lax.rem(place + off % chips, chips)
+
+    def greet_tp(d, carry):
+        greet((me, lax.rem(mine + d, tp_count)))
+        return carry
+
+    for off in range(1, reach + 1):
+        greet((2 * chip_at(off) + core, mine))
+        greet((2 * chip_at(-off) + core, mine))
+    greet((partner, mine))
+    lax.fori_loop(1, tp_count, greet_tp, 0)
+
+    smalls = [
+        pltpu.make_async_copy(source, target, small_sem.at[at])
+        for at, (source, target) in enumerate(
+            (
+                (query_weight_hbm, query_weight_ref),
+                (out_weight_hbm, out_weight_ref),
+                (hidden_hbm, hidden_ref),
+                (pre_gain_hbm, pre_gain_ref),
+                (expert_ids_hbm, expert_ids_ref),
+                (route_logits_hbm, route_logits_ref),
+                (lengths_hbm, lengths_ref),
+                (stick_bias_hbm, stick_bias_ref),
+                (post_gain_hbm, post_gain_ref),
+                (ffn_gain_hbm, ffn_gain_ref),
+                (out_gain_hbm, out_gain_ref),
+            )
         )
-        return carry
-
-    def greet_tp(d, carry):
-        pl.semaphore_signal(
-            barrier, inc=1, device_id=(me, lax.rem(mine + d, tp_count)), device_id_type=MESH
-        )
-        return carry
-
-    lax.fori_loop(1, ep_count, greet_ep, 0)
-    lax.fori_loop(1, tp_count, greet_tp, 0)
-
+    ]
     loads = [
         pltpu.make_async_copy(key_hbm, keys, load_sem.at[0]),
         pltpu.make_async_copy(value_hbm, values, load_sem.at[1]),
@@ -137,8 +167,10 @@
         pltpu.make_async_copy(up_hbm.at[0], ups, load_sem.at[3]),
         pltpu.make_async_copy(down_hbm.at[0], downs, load_sem.at[4]),
     ]
-    for load in loads:
+    for load in smalls + loads:
         load.start()
+    for load in smalls:
+        load.wait()
 
     wq = query_weight_ref[...].astype(F32)
     rows_half = wq.shape[0] // 2
@@ -155,36 +187,32 @@
     ).astype(BF16)
 
     own_columns = pl.ds(pl.multiple_of(mine * width, width), width)
-    own_scr[...] = jnp.zeros_like(own_scr)
-    own_scr[0:sequences, :] = hidden_ref[:, own_columns].astype(F32)
-    ids_scr[...] = jnp.full(ids_scr.shape, -1, jnp.int32)
-    ids_scr[0:sequences, :] = expert_ids_ref[...]
-    logits_scr[...] = jnp.zeros_like(logits_scr)
-    logits_scr[0:sequences, :] = route_logits_ref[...]
+    own_scr[...] = hidden_ref[:, own_columns].astype(F32)
     scores_scr[...] = jnp.zeros_like(scores_scr)
     post_gain = post_gain_ref[...].astype(F32).reshape(1, features)
     for c in range(tp_count):
         gain_scr[c] = post_gain[:, width * c : width * c + width]
 
-    ids = ids_scr[...]
-    lanes = iota((padded, ep_count), 1)
-    picks = [(ids[:, k : k + 1] == lanes).astype(F32) for k in range(2)]
+    ids = expert_ids_ref[...]
+    names = iota((ep_count, sequences), 0)
+    picks = [(ids[k : k + 1, :] == names).astype(F32) for k in range(2)]
     either = picks[0] + picks[1]
-    before = (iota((padded, padded), 1) < iota((padded, padded), 0)).astype(BF16)
-    earlier = jnp.dot(before, either.astype(BF16), preferred_element_type=F32)
-    logits = logits_scr[...]
-    first, second = logits[:, 0:1], logits[:, 1:2]
+    before = (iota((sequences, sequences), 0) < iota((sequences, sequences), 1)).astype(BF16)
+    earlier = jnp.dot(either.astype(BF16), before, preferred_element_type=F32)
+    logits = route_logits_ref[...]
+    first, second = logits[0:1, :], logits[1:2, :]
     top = jnp.maximum(first, second)
     first, second = jnp.exp(first - top), jnp.exp(second - top)
     weighted = picks[0] * (first / (first + second)) + picks[1] * (second / (first + second))
     for s in range(2):
         at_slot = (earlier == float(s)).astype(F32)
-        place_scr[s] = transposed(either * at_slot)
-        mix_scr[s] = weighted * at_slot
+        place_scr[s] = (either * at_slot).astype(BF16)
+        for part, value in enumerate(three_parts(weighted * at_slot)):
+            mix_scr[s, part] = transposed(value).astype(BF16)
 
     for s in range(2):
         hz_out[:, s, :] = jnp.dot(
-            place_scr[s].astype(BF16), own_scr[...].astype(BF16), preferred_element_type=F32
+            place_scr[s], own_scr[...].astype(BF16), preferred_element_type=F32
         )
 
     tri_scr[:, 0:128] = (iota((128, 128), 0) > iota((128, 128), 1)).astype(BF16)
@@ -195,7 +223,7 @@
     for b in range(sequences):
         length_of = jnp.where(row_of == b, lengths_ref[b], length_of)
 
-    pl.semaphore_wait(barrier, ep_count + tp_count - 2)
+    pl.semaphore_wait(barrier, 2 * reach + tp_count)
 
     def far_first(step):
         odd = lax.rem(step, 2)
@@ -222,12 +250,30 @@
             device_id_type=MESH,
         )
 
-    def send_along(copy, recv, slot):
-        def step(s, carry):
-            copy(me, 2 * far_first(s) + core, recv.at[place], slot).start()
-            return carry
-
-        lax.fori_loop(0, chips - 1, step, 0)
+    def send_near(copy, recv, slot):
+        for off in range(reach, 0, -1):
+            copy(me, 2 * chip_at(off) + core, recv.at[place], slot).start()
+            copy(me, 2 * chip_at(-off) + core, recv.at[place], slot).start()
+
+    def send_on(copy, recv, slot):
+        for sign, count in ((1, reach), (-1, reach - 1)):
+            source = chip_at(-sign * reach)
+            owner = 2 * source + core
+            copy(owner, partner, recv.at[source], slot).wait_recv()
+            for off in range(count, 0, -1):
+                copy(owner, 2 * chip_at(sign * off) + core, recv.at[source], slot).start()
+
+    def hand_over(copy, recv, slot, offs, waited):
+        for off in offs:
+            source = chip_at(off)
+            owner = 2 * source + core
+            if off not in waited:
+                copy(owner, partner, recv.at[source], slot).wait_recv()
+            copy(owner, partner, recv_sem.at[slot], slot).start()
+
+    edge = (-reach, reach)
+    near = edge + tuple(sign * off for off in range(reach - 1, 0, -1) for sign in (-1, 1))
+    far = tuple(sign * off for off in range(reach + 1, half) for sign in (-1, 1)) + (half,)
 
     def z_exchange(source, target_ref, sem_at):
         def step(s, carry):
@@ -274,25 +320,15 @@
     WQ_RELAY, WO_RELAY, HZ, HR, RS, ASQ, AZ, AR, EX, BACK, CSQ = range(11)
     WQ_SEND, WO_SEND = 11, 12
 
-    send_along(wq_copy, wq_recv, WQ_SEND)
+    send_near(wq_copy, wq_recv, WQ_SEND)
+    send_near(wo_copy, wo_recv, WO_SEND)
     wq_copy(me, partner, recv_sem.at[WQ_RELAY], WQ_RELAY).start()
-    send_along(wo_copy, wo_recv, WO_SEND)
     wo_copy(me, partner, recv_sem.at[WO_RELAY], WO_RELAY).start()
-    z_exchange(hz_out, hz_in, HZ)
-
-    def relay(copy, recv, slot):
-        def step(d, carry):
-            off = (d + 1) // 2
-            odd = lax.rem(d, 2)
-            source = lax.rem(place + odd * off + (1 - odd) * (chips - off), chips)
-            owner = 2 * source + core
-            copy(owner, partner, recv.at[source], slot).wait_recv()
-            copy(owner, partner, recv_sem.at[slot], slot).start()
-            return carry
-
-        lax.fori_loop(1, chips, step, 0)
-
-    relay(wq_copy, wq_recv, WQ_RELAY)
+    send_on(wq_copy, wq_recv, WQ_SEND)
+    send_on(wo_copy, wo_recv, WO_SEND)
+    hand_over(wq_copy, wq_recv, WQ_RELAY, near, edge)
+    hand_over(wo_copy, wo_recv, WO_RELAY, near, edge)
+    hand_over(wq_copy, wq_recv, WQ_RELAY, far, ())
     bytes_of(wq_all.at[:, 0], chips, recv_sem.at[WQ_RELAY])
 
     for i in range(ep_count):
@@ -345,7 +381,7 @@
         )
     mixed = transposed(mixed_columns).astype(BF16)
 
-    relay(wo_copy, wo_recv, WO_RELAY)
+    hand_over(wo_copy, wo_recv, WO_RELAY, far, ())
     bytes_of(wo_all, chips, recv_sem.at[WO_RELAY])
     left = iota((wo_half, 128), 1) < 64
     for c in range(chips):
@@ -361,26 +397,22 @@
         ).astype(BF16)
     tp_exchange(rs_out, rs_in, RS, True)
     rs_in[mine] = rs_out[mine]
-
-    bytes_of(hz_in, ep_count - 1, recv_sem.at[HZ])
-    hz_in[me] = hz_out[me]
-    h_rows[mine] = jnp.concatenate([hz_in[:, 0, :], hz_in[:, 1, :]], axis=0).astype(BF16)
-    tp_exchange(h_rows, h_rows, HR, False)
+    z_exchange(hz_out, hz_in, HZ)
 
     bytes_of(rs_in, tp_count - 1, recv_sem.at[RS])
     total = rs_in[0].astype(F32)
     for c in range(1, tp_count):
         total = total + rs_in[c].astype(F32)
-    attended = total.astype(BF16)
+    attended = total[0:sequences].astype(BF16)
 
     for s in range(2):
         az_out[:, s, :] = jnp.dot(
-            place_scr[s].astype(BF16), attended, preferred_element_type=F32
+            place_scr[s], attended, preferred_element_type=F32
         )
     z_exchange(az_out, az_in, AZ)
     az_in[me] = az_out[me]
 
-    diagonal = iota((padded, 128), 0) == iota((padded, 128), 1)
+    diagonal = iota((sequences, 128), 0) == iota((sequences, 128), 1)
 
     def as_row(value):
         return jnp.sum(
@@ -395,7 +427,11 @@
     attended = attended.astype(F32)
     asq_in[mine] = as_row(attended)
     tp_exchange(asq_in, asq_in, ASQ, False)
-    bytes_of(h_rows, tp_count - 1, recv_sem.at[HR])
+
+    bytes_of(hz_in, ep_count - 1, recv_sem.at[HZ])
+    hz_in[me] = hz_out[me]
+    h_rows[mine] = jnp.concatenate([hz_in[:, 0, :], hz_in[:, 1, :]], axis=0).astype(BF16)
+    tp_exchange(h_rows, h_rows, HR, False)
 
     bytes_of(az_in, ep_count - 1, recv_sem.at[AZ])
     a_rows[mine] = jnp.concatenate([az_in[:, 0, :], az_in[:, 1, :]], axis=0).astype(BF16)
@@ -412,6 +448,7 @@
     for load in loads[2:]:
         load.wait()
 
+    bytes_of(h_rows, tp_count - 1, recv_sem.at[HR])
     bytes_of(a_rows, tp_count - 1, recv_sem.at[AR])
     rows = 2 * ep_count
     post_gain = post_gain_ref[...].astype(F32).reshape(1, features)
@@ -455,11 +492,11 @@
     z_exchange(back_out, back_in, BACK)
     back_in[me] = back_out[me]
     bytes_of(back_in, ep_count - 1, recv_sem.at[BACK])
-    combined = jnp.zeros((padded, width), F32)
+    combined = jnp.zeros((sequences, width), F32)
     for s in range(2):
         table = back_in[:, s, :].astype(BF16)
-        for part in reversed(three_parts(mix_scr[s])):
-            combined = combined + jnp.dot(part, table, preferred_element_type=F32)
+        for part in (2, 1, 0):
+            combined = combined + jnp.dot(mix_scr[s, part], table, preferred_element_type=F32)
 
     csq_in[mine] = as_row(combined)
     tp_exchange(csq_in, csq_in, CSQ, False)
@@ -483,7 +520,7 @@
     squares = as_column(jnp.sum(csq_in[:, 0, :], axis=0, keepdims=True))
     out_gain = out_gain_ref[...].astype(F32).reshape(1, width)
     result = own_scr[...] + combined * inverse_rms(squares, features) * out_gain
-    result_ref[...] = result[0:sequences].astype(BF16)
+    result_ref[...] = result.astype(BF16)
     bytes_of(csq_in, tp_count - 1, send_sem.at[CSQ])
 
 
@@ -508,14 +545,31 @@
     ep_count = lax.axis_size("ep")
     tp_count = lax.axis_size("tp")
     sequences, features = hidden.shape
+    expert_ids, route_logits = expert_ids.T, route_logits.T
     positions = key_cache.shape[2]
     width = features // tp_count
     chips = ep_count // 2
     rows = 2 * ep_count
-    vmem = pl.BlockSpec(memory_space=pltpu.VMEM)
-    smem = pl.BlockSpec(memory_space=pltpu.SMEM)
-    hbm = pl.BlockSpec(memory_space=pl.ANY)
+    small_args = (
+        hidden,
+        pre_gain,
+        query_weight,
+        lengths,
+        stick_bias,
+        out_weight,
+        post_gain,
+        ffn_gain,
+        expert_ids,
+        route_logits,
+        out_gain,
+    )
     scratch = [
+        *(
+            (pltpu.SMEM if arg is lengths or arg is stick_bias else pltpu.VMEM)(
+                arg.shape, arg.dtype
+            )
+            for arg in small_args
+        ),
         pltpu.VMEM(key_cache.shape, BF16),
         pltpu.VMEM(value_cache.shape, BF16),
         pltpu.VMEM(gate_experts.shape[1:], BF16),
@@ -526,11 +580,9 @@
         pltpu.VMEM((64, features), BF16),
         pltpu.VMEM((16, positions), F32),
         pltpu.VMEM((16, positions), BF16),
-        pltpu.VMEM((2, ep_count, 16), F32),
-        pltpu.VMEM((2, 16, ep_count), F32),
-        pltpu.VMEM((16, 2), jnp.int32),
-        pltpu.VMEM((16, 2), F32),
-        pltpu.VMEM((16, width), F32),
+        pltpu.VMEM((2, ep_count, sequences), BF16),
+        pltpu.VMEM((2, 3, sequences, ep_count), BF16),
+        pltpu.VMEM((sequences, width), F32),
         pltpu.VMEM((tp_count, 1, width), F32),
         pltpu.VMEM((128, 256), BF16),
         pltpu.VMEM((tp_count, 16, width), BF16),
@@ -550,6 +602,7 @@
         pltpu.VMEM((tp_count, 1, width), F32),
         pltpu.VMEM((tp_count, 1, width), F32),
         pltpu.SemaphoreType.DMA((5,)),
+        pltpu.SemaphoreType.DMA((11,)),
         pltpu.SemaphoreType.DMA((chips,)),
         pltpu.SemaphoreType.DMA((chips,)),
         pltpu.SemaphoreType.DMA((13,)),
@@ -558,25 +611,8 @@
     return pl.pallas_call(
         functools.partial(layer_kernel, ep_count, tp_count),
         out_shape=jax.ShapeDtypeStruct((sequences, width), BF16),
-        in_specs=[
-            vmem,
-            vmem,
-            vmem,
-            hbm,
-            hbm,
-            smem,
-            smem,
-            vmem,
-            vmem,
-            vmem,
-            vmem,
-            vmem,
-            hbm,
-            hbm,
-            hbm,
-            vmem,
-        ],
-        out_specs=vmem,
+        in_specs=[pl.BlockSpec(memory_space=pl.ANY)] * 16,
+        out_specs=pl.BlockSpec(memory_space=pltpu.VMEM),
         scratch_shapes=scratch,
         compiler_params=pltpu.CompilerParams(collective_id=0, has_side_effects=True),
         name="layer",

time: 75.7 us -> 69.5 us (0.918)
  Pallas kernels: 70.8 us -> 67.3 us
  local copies, waits for them, and re-layouts: 3.97 us -> 1.28 us
    pallas_call x1, Pallas kernels: 70.8 us -> 67.3 us  [per_device(): pl.pallas_call(functools.partial(layer_kernel, ep_count, tp_count), out_s...]
    unnamed x3 -> x1, local copies, waits for them, and re-layouts: 3.97 us -> 1.28 us
where the time goes in v2:
time: 69.5 us; the launch traced here: 69.2 us
  Pallas kernels  67.3 us (97%)
  local copies, waits for them, and re-layouts  1.28 us (2%)
    pallas_call x1, Pallas kernels, per_device(): pl.pallas_call(functools.partial(layer_kernel, ep_count, tp_count), out_s...  67.3 us

profile of v2, /device:TPU:1, one launch (start us, length us, event | category | flops | bytes accessed | tf_op | source)
XLA Modules:
  0.0 69.2 jit_solution(4216211425360918562)
XLA Ops:
  0.7 67.3 %layer.1 = bf16[12,128]{1,0:T(8,128)(2,1)} custom-call(bf16[12,2048]{1,0:T(8,128)(2,1)} %hidden_hbm.1, bf16[2048]{0:T(1024)(128)(2,1)} %pre_gain_hbm.1, bf16[64,64]{1,0:T(8,128)(2,1)} %query_weight_hbm.1, bf16[12,64,1024]{2,1,0:T(8,128)(2,1)} %key_hbm.1, bf16[12,64,1024]{2,1,0:T(8,128)(2,1)} %value_hbm.1, s32[12]{0:T(128)} %lengths_hbm.1, ...), custom_call_target="tpu_custom_call" | custom-call | tf_op jit(solution)/shard_map/layer/pallas_call | solution.py:611
  67.9 1.3 %copy.19 = bf16[12,128]{1,0:T(8,128)(2,1)} copy(bf16[12,128]{1,0:T(8,128)(2,1)} %layer.1) | data formatting | bytes 6144

commit v3 on v2

--- a/solution.py
+++ b/solution.py
@@ -132,15 +132,22 @@
     def chip_at(off):
         return lax.rem(place + off % chips, chips)
 
-    def greet_tp(d, carry):
-        greet((me, lax.rem(mine + d, tp_count)))
-        return carry
+    side = 4
+    line, spot = mine // side, lax.rem(mine, side)
+    steps = sorted(
+        ((dy, dx) for dy in range(side) for dx in range(side) if dy + dx > 0),
+        key=lambda step: -sum(min(d, side - d) for d in step),
+    )
+    others = [
+        lax.rem(line + dy, side) * side + lax.rem(spot + dx, side) for dy, dx in steps
+    ]
 
     for off in range(1, reach + 1):
         greet((2 * chip_at(off) + core, mine))
         greet((2 * chip_at(-off) + core, mine))
     greet((partner, mine))
-    lax.fori_loop(1, tp_count, greet_tp, 0)
+    for to in others:
+        greet((me, to))
 
     smalls = [
         pltpu.make_async_copy(source, target, small_sem.at[at])
@@ -169,7 +176,7 @@
     ]
     for load in smalls + loads:
         load.start()
-    for load in smalls:
+    for load in smalls[:2]:
         load.wait()
 
     wq = query_weight_ref[...].astype(F32)
@@ -179,6 +186,113 @@
     wo_half = wo.shape[0] // 2
     wo_all[me] = jnp.concatenate([wo[:wo_half], wo[wo_half:]], axis=1).astype(BF16)
 
+    pl.semaphore_wait(barrier, 2 * reach + tp_count)
+
+    def wq_copy(owner, target, sem, slot):
+        return pltpu.make_async_remote_copy(
+            src_ref=wq_all.at[owner, 0],
+            dst_ref=wq_all.at[owner, 0],
+            send_sem=send_sem.at[slot],
+            recv_sem=sem,
+            device_id=(target, mine),
+            device_id_type=MESH,
+        )
+
+    def wo_copy(owner, target, sem, slot):
+        return pltpu.make_async_remote_copy(
+            src_ref=wo_all.at[owner],
+            dst_ref=wo_all.at[owner],
+            send_sem=send_sem.at[slot],
+            recv_sem=sem,
+            device_id=(target, mine),
+            device_id_type=MESH,
+        )
+
+    def send_near(copy, recv, slot):
+        for off in range(reach, 0, -1):
+            copy(me, 2 * chip_at(off) + core, recv.at[place], slot).start()
+            copy(me, 2 * chip_at(-off) + core, recv.at[place], slot).start()
+
+    def send_on(copy, recv, slot):
+        for sign, count in ((1, reach), (-1, reach - 1)):
+            source = chip_at(-sign * reach)
+            owner = 2 * source + core
+            copy(owner, partner, recv.at[source], slot).wait_recv()
+            for off in range(count, 0, -1):
+                copy(owner, 2 * chip_at(sign * off) + core, recv.at[source], slot).start()
+
+    def hand_over(copy, recv, slot, offs, waited):
+        for off in offs:
+            source = chip_at(off)
+            owner = 2 * source + core
+            if off not in waited:
+                copy(owner, partner, recv.at[source], slot).wait_recv()
+            copy(owner, partner, recv_sem.at[slot], slot).start()
+
+    edge = (-reach, reach)
+    near = edge + tuple(sign * off for off in range(reach - 1, 0, -1) for sign in (-1, 1))
+    far = tuple(sign * off for off in range(reach + 1, half) for sign in (-1, 1)) + (half,)
+
+    def z_send(source, target, send_at, recv_at, off, other):
+        to = 2 * chip_at(off) + other
+        pltpu.make_async_remote_copy(
+            src_ref=source(to, off, other),
+            dst_ref=target(off),
+            send_sem=send_sem.at[send_at],
+            recv_sem=recv_sem.at[recv_at],
+            device_id=(to, mine),
+            device_id_type=MESH,
+        ).start()
+
+    def z_offs(offs):
+        return sorted(offs, key=lambda off: -min(off % chips, -off % chips))
+
+    def z_all(source, target, send_at, recv_of, offs):
+        for off in z_offs(offs):
+            if off == 0:
+                z_send(source, target, send_at, recv_of(off), off, 1 - core)
+            else:
+                for other in range(2):
+                    z_send(source, target, send_at, recv_of(off), off, other)
+
+    def spread(source, target, send_at, recv_at):
+        z_all(
+            lambda to, off, other: source.at[to],
+            lambda off: target.at[2 * ((reach - off) % chips) + core],
+            send_at,
+            lambda off: recv_at[(reach - off) % chips // half],
+            range(chips),
+        )
+        target[2 * reach + core] = source[me]
+
+    def rows_of(arrived, at):
+        part = slice(ep_count // 2 * at, ep_count // 2 * (at + 1))
+        return jnp.concatenate([arrived[part, 0, :], arrived[part, 1, :]], axis=0).astype(BF16)
+
+    def tp_exchange(source, target_ref, sem_at, scatter):
+        for to in others:
+            pltpu.make_async_remote_copy(
+                src_ref=source.at[to] if scatter else source.at[mine],
+                dst_ref=target_ref.at[mine],
+                send_sem=send_sem.at[sem_at],
+                recv_sem=recv_sem.at[sem_at],
+                device_id=(me, to),
+                device_id_type=MESH,
+            ).start()
+
+    def bytes_of(ref, count, sem):
+        some = ref.at[pl.ds(0, count)]
+        pltpu.make_async_copy(some, some, sem).wait()
+
+    WQ_RELAY, WO_RELAY, WQ_SEND, WO_SEND, HZ, HR, RS, ASQ, BACK, CSQ = range(10)
+    AZ, AR, EX = (10, 11), (12, 13), (14, 15)
+
+    send_near(wq_copy, wq_recv, WQ_SEND)
+    send_near(wo_copy, wo_recv, WO_SEND)
+    wq_copy(me, partner, recv_sem.at[WQ_RELAY], WQ_RELAY).start()
+    wo_copy(me, partner, recv_sem.at[WO_RELAY], WO_RELAY).start()
+    for load in smalls[2:]:
+        load.wait()
     hidden = hidden_ref[...].astype(F32)
     normed = (
         hidden
@@ -223,107 +337,6 @@
     for b in range(sequences):
         length_of = jnp.where(row_of == b, lengths_ref[b], length_of)
 
-    pl.semaphore_wait(barrier, 2 * reach + tp_count)
-
-    def far_first(step):
-        odd = lax.rem(step, 2)
-        off = half + (1 - odd) * (step // 2) - odd * ((step + 1) // 2)
-        return lax.rem(place + off, chips)
-
-    def wq_copy(owner, target, sem, slot):
-        return pltpu.make_async_remote_copy(
-            src_ref=wq_all.at[owner, 0],
-            dst_ref=wq_all.at[owner, 0],
-            send_sem=send_sem.at[slot],
-            recv_sem=sem,
-            device_id=(target, mine),
-            device_id_type=MESH,
-        )
-
-    def wo_copy(owner, target, sem, slot):
-        return pltpu.make_async_remote_copy(
-            src_ref=wo_all.at[owner],
-            dst_ref=wo_all.at[owner],
-            send_sem=send_sem.at[slot],
-            recv_sem=sem,
-            device_id=(target, mine),
-            device_id_type=MESH,
-        )
-
-    def send_near(copy, recv, slot):
-        for off in range(reach, 0, -1):
-            copy(me, 2 * chip_at(off) + core, recv.at[place], slot).start()
-            copy(me, 2 * chip_at(-off) + core, recv.at[place], slot).start()
-
-    def send_on(copy, recv, slot):
-        for sign, count in ((1, reach), (-1, reach - 1)):
-            source = chip_at(-sign * reach)
-            owner = 2 * source + core
-            copy(owner, partner, recv.at[source], slot).wait_recv()
-            for off in range(count, 0, -1):
-                copy(owner, 2 * chip_at(sign * off) + core, recv.at[source], slot).start()
-
-    def hand_over(copy, recv, slot, offs, waited):
-        for off in offs:
-            source = chip_at(off)
-            owner = 2 * source + core
-            if off not in waited:
-                copy(owner, partner, recv.at[source], slot).wait_recv()
-            copy(owner, partner, recv_sem.at[slot], slot).start()
-
-    edge = (-reach, reach)
-    near = edge + tuple(sign * off for off in range(reach - 1, 0, -1) for sign in (-1, 1))
-    far = tuple(sign * off for off in range(reach + 1, half) for sign in (-1, 1)) + (half,)
-
-    def z_exchange(source, target_ref, sem_at):
-        def step(s, carry):
-            to = 2 * far_first(s // 2) + lax.rem(s, 2)
-            pltpu.make_async_remote_copy(
-                src_ref=source.at[to],
-                dst_ref=target_ref.at[me],
-                send_sem=send_sem.at[sem_at],
-                recv_sem=recv_sem.at[sem_at],
-                device_id=(to, mine),
-                device_id_type=MESH,
-            ).start()
-            return carry
-
-        lax.fori_loop(0, 2 * (chips - 1), step, 0)
-        pltpu.make_async_remote_copy(
-            src_ref=source.at[partner],
-            dst_ref=target_ref.at[me],
-            send_sem=send_sem.at[sem_at],
-            recv_sem=recv_sem.at[sem_at],
-            device_id=(partner, mine),
-            device_id_type=MESH,
-        ).start()
-
-    def tp_exchange(source, target_ref, sem_at, scatter):
-        def step(d, carry):
-            to = lax.rem(mine + d, tp_count)
-            pltpu.make_async_remote_copy(
-                src_ref=source.at[to] if scatter else source.at[mine],
-                dst_ref=target_ref.at[mine],
-                send_sem=send_sem.at[sem_at],
-                recv_sem=recv_sem.at[sem_at],
-                device_id=(me, to),
-                device_id_type=MESH,
-            ).start()
-            return carry
-
-        lax.fori_loop(1, tp_count, step, 0)
-
-    def bytes_of(ref, count, sem):
-        some = ref.at[pl.ds(0, count)]
-        pltpu.make_async_copy(some, some, sem).wait()
-
-    WQ_RELAY, WO_RELAY, HZ, HR, RS, ASQ, AZ, AR, EX, BACK, CSQ = range(11)
-    WQ_SEND, WO_SEND = 11, 12
-
-    send_near(wq_copy, wq_recv, WQ_SEND)
-    send_near(wo_copy, wo_recv, WO_SEND)
-    wq_copy(me, partner, recv_sem.at[WQ_RELAY], WQ_RELAY).start()
-    wo_copy(me, partner, recv_sem.at[WO_RELAY], WO_RELAY).start()
     send_on(wq_copy, wq_recv, WQ_SEND)
     send_on(wo_copy, wo_recv, WO_SEND)
     hand_over(wq_copy, wq_recv, WQ_RELAY, near, edge)
@@ -342,6 +355,7 @@
     for b in range(sequences):
         product = keys[b].astype(F32) * query_columns[:, b : b + 1]
         scores_scr[b : b + 1, :] = jnp.sum(product, axis=0, keepdims=True)
+    hand_over(wo_copy, wo_recv, WO_RELAY, far, ())
     bias = stick_bias_ref[0]
     fails, log_hits, insides = [], [], []
     for c in range(blocks):
@@ -381,7 +395,7 @@
         )
     mixed = transposed(mixed_columns).astype(BF16)
 
-    hand_over(wo_copy, wo_recv, WO_RELAY, far, ())
+    spread(hz_out, hz_in, HZ, (HZ, HZ))
     bytes_of(wo_all, chips, recv_sem.at[WO_RELAY])
     left = iota((wo_half, 128), 1) < 64
     for c in range(chips):
@@ -397,7 +411,6 @@
         ).astype(BF16)
     tp_exchange(rs_out, rs_in, RS, True)
     rs_in[mine] = rs_out[mine]
-    z_exchange(hz_out, hz_in, HZ)
 
     bytes_of(rs_in, tp_count - 1, recv_sem.at[RS])
     total = rs_in[0].astype(F32)
@@ -409,8 +422,7 @@
         az_out[:, s, :] = jnp.dot(
             place_scr[s], attended, preferred_element_type=F32
         )
-    z_exchange(az_out, az_in, AZ)
-    az_in[me] = az_out[me]
+    spread(az_out, az_in, AZ[0], AZ)
 
     diagonal = iota((sequences, 128), 0) == iota((sequences, 128), 1)
 
@@ -429,13 +441,14 @@
     tp_exchange(asq_in, asq_in, ASQ, False)
 
     bytes_of(hz_in, ep_count - 1, recv_sem.at[HZ])
-    hz_in[me] = hz_out[me]
-    h_rows[mine] = jnp.concatenate([hz_in[:, 0, :], hz_in[:, 1, :]], axis=0).astype(BF16)
+    for at in range(2):
+        h_rows[mine, at] = rows_of(hz_in, at)
     tp_exchange(h_rows, h_rows, HR, False)
 
-    bytes_of(az_in, ep_count - 1, recv_sem.at[AZ])
-    a_rows[mine] = jnp.concatenate([az_in[:, 0, :], az_in[:, 1, :]], axis=0).astype(BF16)
-    tp_exchange(a_rows, a_rows, AR, False)
+    for at in range(2):
+        bytes_of(az_in, ep_count // 2 - 1 + at, recv_sem.at[AZ[at]])
+        a_rows[at, mine] = rows_of(az_in, at)
+        tp_exchange(a_rows.at[at], a_rows.at[at], AR[at], False)
 
     bytes_of(asq_in, tp_count - 1, recv_sem.at[ASQ])
     squares = as_column(jnp.sum(asq_in[:, 0, :], axis=0, keepdims=True))
@@ -448,49 +461,64 @@
     for load in loads[2:]:
         load.wait()
 
-    bytes_of(h_rows, tp_count - 1, recv_sem.at[HR])
-    bytes_of(a_rows, tp_count - 1, recv_sem.at[AR])
-    rows = 2 * ep_count
     post_gain = post_gain_ref[...].astype(F32).reshape(1, features)
     ffn_gain = ffn_gain_ref[...].astype(F32).reshape(1, features)
-    square = jnp.zeros((rows, width), F32)
-    for c in range(tp_count):
-        one = a_rows[c].astype(F32)
-        square = square + one * one
-    scale = inverse_rms(jnp.sum(square, axis=1, keepdims=True), features)
-    square = jnp.zeros((rows, width), F32)
-    for c in range(tp_count):
-        columns = slice(width * c, width * c + width)
-        one = (
-            h_rows[c].astype(F32) + a_rows[c].astype(F32) * scale * post_gain[:, columns]
-        ).astype(BF16)
-        r_scr[c] = one
-        one = one.astype(F32)
-        square = square + one * one
-    scale = inverse_rms(jnp.sum(square, axis=1, keepdims=True), features)
-    for c in range(tp_count):
-        columns = slice(width * c, width * c + width)
-        f_scr[:, columns] = (r_scr[c].astype(F32) * scale * ffn_gain[:, columns]).astype(BF16)
-    ffn_in = f_scr[...]
-    gate_act = jnp.dot(ffn_in, gates[...], preferred_element_type=F32)
-    up_act = jnp.dot(ffn_in, ups[...], preferred_element_type=F32)
-    active = (gate_act / (1.0 + jnp.exp(-gate_act)) * up_act).astype(BF16)
-    for c in range(tp_count):
-        ex_out[c] = jnp.dot(
-            active, downs[:, width * c : width * c + width], preferred_element_type=F32
-        ).astype(BF16)
-    tp_exchange(ex_out, ex_in, EX, True)
-    ex_in[mine] = ex_out[mine]
-    bytes_of(ex_in, tp_count - 1, recv_sem.at[EX])
-    total = ex_in[0].astype(F32)
-    for c in range(1, tp_count):
-        total = total + ex_in[c].astype(F32)
-    total = total.astype(BF16).astype(F32)
-
-    for s in range(2):
-        back_out[:, s, :] = total[ep_count * s : ep_count * s + ep_count]
-    z_exchange(back_out, back_in, BACK)
-    back_in[me] = back_out[me]
+
+    def expert(at):
+        square = jnp.zeros((ep_count, width), F32)
+        for c in range(tp_count):
+            one = a_rows[at, c].astype(F32)
+            square = square + one * one
+        scale = inverse_rms(jnp.sum(square, axis=1, keepdims=True), features)
+        square = jnp.zeros((ep_count, width), F32)
+        for c in range(tp_count):
+            columns = slice(width * c, width * c + width)
+            one = (
+                h_rows[c, at].astype(F32)
+                + a_rows[at, c].astype(F32) * scale * post_gain[:, columns]
+            ).astype(BF16)
+            r_scr[at, c] = one
+            one = one.astype(F32)
+            square = square + one * one
+        scale = inverse_rms(jnp.sum(square, axis=1, keepdims=True), features)
+        for c in range(tp_count):
+            columns = slice(width * c, width * c + width)
+            f_scr[at, :, columns] = (
+                r_scr[at, c].astype(F32) * scale * ffn_gain[:, columns]
+            ).astype(BF16)
+        ffn_in = f_scr[at]
+        gate_act = jnp.dot(ffn_in, gates[...], preferred_element_type=F32)
+        up_act = jnp.dot(ffn_in, ups[...], preferred_element_type=F32)
+        active = (gate_act / (1.0 + jnp.exp(-gate_act)) * up_act).astype(BF16)
+        for c in range(tp_count):
+            ex_out[at, c] = jnp.dot(
+                active, downs[:, width * c : width * c + width], preferred_element_type=F32
+            ).astype(BF16)
+        tp_exchange(ex_out.at[at], ex_in.at[at], EX[at], True)
+        ex_in[at, mine] = ex_out[at, mine]
+
+    bytes_of(h_rows, tp_count - 1, recv_sem.at[HR])
+    for at in range(2):
+        bytes_of(a_rows.at[at], tp_count - 1, recv_sem.at[AR[at]])
+        expert(at)
+
+    for at in range(2):
+        bytes_of(ex_in.at[at], tp_count - 1, recv_sem.at[EX[at]])
+        total = ex_in[at, 0].astype(F32)
+        for c in range(1, tp_count):
+            total = total + ex_in[at, c].astype(F32)
+        total = total.astype(BF16).astype(F32)
+        part = slice(ep_count // 2 * at, ep_count // 2 * (at + 1))
+        for s in range(2):
+            back_out[part, s, :] = total[ep_count // 2 * s : ep_count // 2 * (s + 1)]
+        z_all(
+            lambda to, off, other: back_out.at[2 * ((off + reach) % chips) + other],
+            lambda off: back_in.at[me],
+            BACK,
+            lambda off: BACK,
+            [(rel - reach) % chips for rel in range(half * at, half * (at + 1))],
+        )
+    back_in[me] = back_out[2 * reach + core]
     bytes_of(back_in, ep_count - 1, recv_sem.at[BACK])
     combined = jnp.zeros((sequences, width), F32)
     for s in range(2):
@@ -505,14 +533,16 @@
     bytes_of(wq_all.at[:, 0], chips, send_sem.at[WQ_RELAY])
     bytes_of(wo_all, chips - 1, send_sem.at[WO_SEND])
     bytes_of(wo_all, chips, send_sem.at[WO_RELAY])
-    for ref, slot in ((hz_out, HZ), (az_out, AZ), (back_out, BACK)):
+    for ref, slot in ((hz_out, HZ), (az_out, AZ[0]), (back_out, BACK)):
         bytes_of(ref, ep_count - 1, send_sem.at[slot])
     for ref, slot in (
         (rs_out, RS),
         (h_rows, HR),
         (asq_in, ASQ),
-        (a_rows, AR),
-        (ex_out, EX),
+        (a_rows.at[0], AR[0]),
+        (a_rows.at[1], AR[1]),
+        (ex_out.at[0], EX[0]),
+        (ex_out.at[1], EX[1]),
     ):
         bytes_of(ref, tp_count - 1, send_sem.at[slot])
 
@@ -549,7 +579,6 @@
     positions = key_cache.shape[2]
     width = features // tp_count
     chips = ep_count // 2
-    rows = 2 * ep_count
     small_args = (
         hidden,
         pre_gain,
@@ -591,12 +620,12 @@
         pltpu.VMEM((ep_count, 2, width), F32),
         pltpu.VMEM((ep_count, 2, width), F32),
         pltpu.VMEM((ep_count, 2, width), F32),
-        pltpu.VMEM((tp_count, rows, width), BF16),
-        pltpu.VMEM((tp_count, rows, width), BF16),
-        pltpu.VMEM((tp_count, rows, width), BF16),
-        pltpu.VMEM((rows, features), BF16),
-        pltpu.VMEM((tp_count, rows, width), BF16),
-        pltpu.VMEM((tp_count, rows, width), BF16),
+        pltpu.VMEM((tp_count, 2, ep_count, width), BF16),
+        pltpu.VMEM((2, tp_count, ep_count, width), BF16),
+        pltpu.VMEM((2, tp_count, ep_count, width), BF16),
+        pltpu.VMEM((2, ep_count, features), BF16),
+        pltpu.VMEM((2, tp_count, ep_count, width), BF16),
+        pltpu.VMEM((2, tp_count, ep_count, width), BF16),
         pltpu.VMEM((ep_count, 2, width), F32),
         pltpu.VMEM((ep_count, 2, width), F32),
         pltpu.VMEM((tp_count, 1, width), F32),
@@ -605,12 +634,12 @@
         pltpu.SemaphoreType.DMA((11,)),
         pltpu.SemaphoreType.DMA((chips,)),
         pltpu.SemaphoreType.DMA((chips,)),
-        pltpu.SemaphoreType.DMA((13,)),
-        pltpu.SemaphoreType.DMA((13,)),
+        pltpu.SemaphoreType.DMA((16,)),
+        pltpu.SemaphoreType.DMA((16,)),
     ]
     return pl.pallas_call(
         functools.partial(layer_kernel, ep_count, tp_count),
-        out_shape=jax.ShapeDtypeStruct((sequences, width), BF16),
+        out_shape=pltpu.VMEM((sequences, width), BF16),
         in_specs=[pl.BlockSpec(memory_space=pl.ANY)] * 16,
         out_specs=pl.BlockSpec(memory_space=pltpu.VMEM),
         scratch_shapes=scratch,

time: 69.5 us -> 64.2 us (0.924)
  Pallas kernels: 67.3 us -> 62.8 us
    pallas_call x1, Pallas kernels: 67.3 us -> 62.8 us  [per_device(): pl.pallas_call(functools.partial(layer_kernel, ep_count, tp_count), out_s...]
where the time goes in v3:
time: 64.2 us; the launch traced here: 64 us
  Pallas kernels  62.8 us (98%)
  between operations  0.66 us (1%)
    pallas_call x1, Pallas kernels, per_device(): pl.pallas_call(functools.partial(layer_kernel, ep_count, tp_count), out_s...  62.8 us

profile of v3, /device:TPU:1, one launch (start us, length us, event | category | flops | bytes accessed | tf_op | source)
XLA Modules:
  0.0 64.0 jit_solution(13242805080840718043)
XLA Ops:
  0.7 62.8 %layer.1 = bf16[12,128]{1,0:T(8,128)(2,1)S(1)} custom-call(bf16[12,2048]{1,0:T(8,128)(2,1)} %hidden_hbm.1, bf16[2048]{0:T(1024)(128)(2,1)} %pre_gain_hbm.1, bf16[64,64]{1,0:T(8,128)(2,1)} %query_weight_hbm.1, bf16[12,64,1024]{2,1,0:T(8,128)(2,1)} %key_hbm.1, bf16[12,64,1024]{2,1,0:T(8,128)(2,1)} %value_hbm.1, s32[12]{0:T(128)} %lengths_hbm.1, ...), custom_call_target="tpu_custom_call" | custom-call | tf_op jit(solution)/shard_map/layer/pallas_call | solution.py:640
  63.4 0.6 copy.18

commit v4 on v3

--- a/solution.py
+++ b/solution.py
@@ -103,9 +103,7 @@
     asq_in,
     csq_in,
     load_sem,
-    small_sem,
-    wq_recv,
-    wo_recv,
+    weight_sem,
     recv_sem,
     send_sem,
 ):
@@ -133,6 +131,9 @@
         return lax.rem(place + off % chips, chips)
 
     side = 4
+    WQ_RELAY, WO_RELAY, HZ, HR, RS, ASQ, BACK, CSQ = range(8)
+    AZ, AR, EX = (8, 9), (10, 11), (12, 13)
+    WEIGHTS, ROWS, OTHERS = range(3)
     line, spot = mine // side, lax.rem(mine, side)
     steps = sorted(
         ((dy, dx) for dy in range(side) for dx in range(side) if dy + dx > 0),
@@ -150,7 +151,7 @@
         greet((me, to))
 
     smalls = [
-        pltpu.make_async_copy(source, target, small_sem.at[at])
+        pltpu.make_async_copy(source, target, load_sem.at[at])
         for at, (source, target) in enumerate(
             (
                 (query_weight_hbm, query_weight_ref),
@@ -174,71 +175,68 @@
         pltpu.make_async_copy(up_hbm.at[0], ups, load_sem.at[3]),
         pltpu.make_async_copy(down_hbm.at[0], downs, load_sem.at[4]),
     ]
-    for load in smalls + loads:
+    for load in smalls:
         load.start()
     for load in smalls[:2]:
         load.wait()
 
-    wq = query_weight_ref[...].astype(F32)
-    rows_half = wq.shape[0] // 2
-    wq_all[me, 0] = jnp.concatenate([wq[:rows_half], wq[rows_half:]], axis=1).astype(BF16)
-    wo = out_weight_ref[...].astype(F32)
-    wo_half = wo.shape[0] // 2
-    wo_all[me] = jnp.concatenate([wo[:wo_half], wo[wo_half:]], axis=1).astype(BF16)
+    def folded(value):
+        rows = value.shape[0] // 2
+        return jnp.concatenate([value[:rows], value[rows:]], axis=1).astype(BF16)
+
+    wq_all[me, 0] = folded(query_weight_ref[...].astype(F32))
+    wo_all[me] = folded(out_weight_ref[...].astype(F32))
+    wo_half = out_weight_ref.shape[0] // 2
 
     pl.semaphore_wait(barrier, 2 * reach + tp_count)
 
-    def wq_copy(owner, target, sem, slot):
-        return pltpu.make_async_remote_copy(
-            src_ref=wq_all.at[owner, 0],
-            dst_ref=wq_all.at[owner, 0],
-            send_sem=send_sem.at[slot],
-            recv_sem=sem,
-            device_id=(target, mine),
-            device_id_type=MESH,
-        )
-
-    def wo_copy(owner, target, sem, slot):
-        return pltpu.make_async_remote_copy(
-            src_ref=wo_all.at[owner],
-            dst_ref=wo_all.at[owner],
-            send_sem=send_sem.at[slot],
-            recv_sem=sem,
-            device_id=(target, mine),
-            device_id_type=MESH,
-        )
-
-    def send_near(copy, recv, slot):
+    def weight(view, base, relay_at):
+        def copy(owner, target, sem):
+            return pltpu.make_async_remote_copy(
+                src_ref=view(owner),
+                dst_ref=view(owner),
+                send_sem=send_sem.at[WEIGHTS],
+                recv_sem=sem,
+                device_id=(target, mine),
+                device_id_type=MESH,
+            )
+
+        return copy, base, relay_at
+
+    def send_near(kind):
+        copy, base, relay_at = kind
         for off in range(reach, 0, -1):
-            copy(me, 2 * chip_at(off) + core, recv.at[place], slot).start()
-            copy(me, 2 * chip_at(-off) + core, recv.at[place], slot).start()
-
-    def send_on(copy, recv, slot):
-        for sign, count in ((1, reach), (-1, reach - 1)):
-            source = chip_at(-sign * reach)
-            owner = 2 * source + core
-            copy(owner, partner, recv.at[source], slot).wait_recv()
+            edge = off == reach
+            copy(me, 2 * chip_at(off) + core, weight_sem.at[base + (0 if edge else 2)]).start()
+            copy(me, 2 * chip_at(-off) + core, weight_sem.at[base + (1 if edge else 2)]).start()
+
+    def send_on(kind):
+        copy, base, relay_at = kind
+        for way, at, count in (
+            (1 - 2 * core, core, reach),
+            (2 * core - 1, 1 - core, reach - 1),
+        ):
+            owner = 2 * lax.rem(place - way * reach + chips, chips) + core
+            copy(owner, partner, weight_sem.at[base + at]).wait_recv()
             for off in range(count, 0, -1):
-                copy(owner, 2 * chip_at(sign * off) + core, recv.at[source], slot).start()
-
-    def hand_over(copy, recv, slot, offs, waited):
+                to = lax.rem(place + way * off + chips, chips)
+                copy(owner, 2 * to + core, weight_sem.at[base + 3]).start()
+
+    def hand_over(kind, offs):
+        copy, base, relay_at = kind
         for off in offs:
-            source = chip_at(off)
-            owner = 2 * source + core
-            if off not in waited:
-                copy(owner, partner, recv.at[source], slot).wait_recv()
-            copy(owner, partner, recv_sem.at[slot], slot).start()
-
-    edge = (-reach, reach)
-    near = edge + tuple(sign * off for off in range(reach - 1, 0, -1) for sign in (-1, 1))
+            copy(2 * chip_at(off) + core, partner, recv_sem.at[relay_at]).start()
+
+    inner = 2 * (reach - 1)
+    near = tuple(sign * off for off in range(reach, 0, -1) for sign in (-1, 1))
     far = tuple(sign * off for off in range(reach + 1, half) for sign in (-1, 1)) + (half,)
 
-    def z_send(source, target, send_at, recv_at, off, other):
+    def z_send(source, target, recv_at, off, other):
         to = 2 * chip_at(off) + other
         pltpu.make_async_remote_copy(
             src_ref=source(to, off, other),
             dst_ref=target(off),
-            send_sem=send_sem.at[send_at],
+            send_sem=send_sem.at[OTHERS],
             recv_sem=recv_sem.at[recv_at],
             device_id=(to, mine),
             device_id_type=MESH,
@@ -247,19 +245,18 @@
     def z_offs(offs):
         return sorted(offs, key=lambda off: -min(off % chips, -off % chips))
 
-    def z_all(source, target, send_at, recv_of, offs):
+    def z_all(source, target, recv_of, offs):
         for off in z_offs(offs):
             if off == 0:
-                z_send(source, target, send_at, recv_of(off), off, 1 - core)
+                z_send(source, target, recv_of(off), off, 1 - core)
             else:
                 for other in range(2):
-                    z_send(source, target, send_at, recv_of(off), off, other)
-
-    def spread(source, target, send_at, recv_at):
+                    z_send(source, target, recv_of(off), off, other)
+
+    def spread(source, target, recv_at):
         z_all(
             lambda to, off, other: source.at[to],
             lambda off: target.at[2 * ((reach - off) % chips) + core],
-            send_at,
             lambda off: recv_at[(reach - off) % chips // half],
             range(chips),
         )
@@ -269,12 +266,12 @@
         part = slice(ep_count // 2 * at, ep_count // 2 * (at + 1))
         return jnp.concatenate([arrived[part, 0, :], arrived[part, 1, :]], axis=0).astype(BF16)
 
-    def tp_exchange(source, target_ref, sem_at, scatter):
+    def tp_exchange(source, target_ref, sem_at, scatter, send_at):
         for to in others:
             pltpu.make_async_remote_copy(
                 src_ref=source.at[to] if scatter else source.at[mine],
                 dst_ref=target_ref.at[mine],
-                send_sem=send_sem.at[sem_at],
+                send_sem=send_sem.at[send_at],
                 recv_sem=recv_sem.at[sem_at],
                 device_id=(me, to),
                 device_id_type=MESH,
@@ -284,15 +281,17 @@
         some = ref.at[pl.ds(0, count)]
         pltpu.make_async_copy(some, some, sem).wait()
 
-    WQ_RELAY, WO_RELAY, WQ_SEND, WO_SEND, HZ, HR, RS, ASQ, BACK, CSQ = range(10)
-    AZ, AR, EX = (10, 11), (12, 13), (14, 15)
-
-    send_near(wq_copy, wq_recv, WQ_SEND)
-    send_near(wo_copy, wo_recv, WO_SEND)
-    wq_copy(me, partner, recv_sem.at[WQ_RELAY], WQ_RELAY).start()
-    wo_copy(me, partner, recv_sem.at[WO_RELAY], WO_RELAY).start()
+    wq = weight(lambda owner: wq_all.at[owner, 0], 0, WQ_RELAY)
+    wo = weight(lambda owner: wo_all.at[owner], 4, WO_RELAY)
+
+    send_near(wq)
+    send_near(wo)
+    hand_over(wq, (0,))
+    hand_over(wo, (0,))
     for load in smalls[2:]:
         load.wait()
+    for load in loads:
+        load.start()
     hidden = hidden_ref[...].astype(F32)
     normed = (
         hidden
@@ -337,12 +336,16 @@
     for b in range(sequences):
         length_of = jnp.where(row_of == b, lengths_ref[b], length_of)
 
-    send_on(wq_copy, wq_recv, WQ_SEND)
-    send_on(wo_copy, wo_recv, WO_SEND)
-    hand_over(wq_copy, wq_recv, WQ_RELAY, near, edge)
-    hand_over(wo_copy, wo_recv, WO_RELAY, near, edge)
-    hand_over(wq_copy, wq_recv, WQ_RELAY, far, ())
+    send_on(wq)
+    send_on(wo)
+    bytes_of(wq_all.at[:, 0], inner, weight_sem.at[2])
+    hand_over(wq, near)
+    bytes_of(wo_all, inner, weight_sem.at[6])
+    hand_over(wo, near)
+    bytes_of(wq_all.at[:, 0], len(far), weight_sem.at[3])
+    hand_over(wq, far)
     bytes_of(wq_all.at[:, 0], chips, recv_sem.at[WQ_RELAY])
+    spread(hz_out, hz_in, (HZ, HZ))
 
     for i in range(ep_count):
         wq_all[i, 1] = pltpu.roll(wq_all[i, 0].astype(F32), 64, 1).astype(BF16)
@@ -351,11 +354,13 @@
     )[:, 0:head_size]
     query_columns = transposed(queries)
 
+    bytes_of(wo_all, len(far), weight_sem.at[7])
+    hand_over(wo, far)
+
     loads[0].wait()
     for b in range(sequences):
         product = keys[b].astype(F32) * query_columns[:, b : b + 1]
         scores_scr[b : b + 1, :] = jnp.sum(product, axis=0, keepdims=True)
-    hand_over(wo_copy, wo_recv, WO_RELAY, far, ())
     bias = stick_bias_ref[0]
     fails, log_hits, insides = [], [], []
     for c in range(blocks):
@@ -377,25 +382,22 @@
         after = block[:, 0:128] + later
         stick_scr[:, 128 * c : 128 * c + 128] = jnp.where(
             insides[c], jnp.exp(log_hits[c] + after), 0.0
-        ).astype(BF16)
+        ).astype(BF16).astype(F32)
         later = later + block[:, 128:256]
 
     loads[1].wait()
-    read = lax.dot_general(
-        values[...].reshape(sequences * head_size, positions),
-        stick_scr[...],
-        NT,
-        preferred_element_type=F32,
-    )
     column = iota((head_size, padded), 1)
     mixed_columns = jnp.zeros((head_size, padded), F32)
     for b in range(sequences):
+        read = jnp.zeros((head_size, 128), F32)
+        for c in range(blocks):
+            columns = slice(128 * c, 128 * c + 128)
+            read = read + values[b, :, columns].astype(F32) * stick_scr[b : b + 1, columns]
         mixed_columns = jnp.where(
-            column == b, read[head_size * b : head_size * b + head_size], mixed_columns
+            column == b, jnp.sum(read, axis=1, keepdims=True), mixed_columns
         )
     mixed = transposed(mixed_columns).astype(BF16)
 
-    spread(hz_out, hz_in, HZ, (HZ, HZ))
     bytes_of(wo_all, chips, recv_sem.at[WO_RELAY])
     left = iota((wo_half, 128), 1) < 64
     for c in range(chips):
@@ -409,7 +411,7 @@
         rs_out[c] = jnp.dot(
             mixed, wo_full[:, width * c : width * c + width], preferred_element_type=F32
         ).astype(BF16)
-    tp_exchange(rs_out, rs_in, RS, True)
+    tp_exchange(rs_out, rs_in, RS, True, OTHERS)
     rs_in[mine] = rs_out[mine]
 
     bytes_of(rs_in, tp_count - 1, recv_sem.at[RS])
@@ -422,7 +424,7 @@
         az_out[:, s, :] = jnp.dot(
             place_scr[s], attended, preferred_element_type=F32
         )
-    spread(az_out, az_in, AZ[0], AZ)
+    spread(az_out, az_in, AZ)
 
     diagonal = iota((sequences, 128), 0) == iota((sequences, 128), 1)
 
@@ -438,17 +440,17 @@
 
     attended = attended.astype(F32)
     asq_in[mine] = as_row(attended)
-    tp_exchange(asq_in, asq_in, ASQ, False)
+    tp_exchange(asq_in, asq_in, ASQ, False, OTHERS)
 
     bytes_of(hz_in, ep_count - 1, recv_sem.at[HZ])
     for at in range(2):
         h_rows[mine, at] = rows_of(hz_in, at)
-    tp_exchange(h_rows, h_rows, HR, False)
+    tp_exchange(h_rows, h_rows, HR, False, ROWS)
 
     for at in range(2):
         bytes_of(az_in, ep_count // 2 - 1 + at, recv_sem.at[AZ[at]])
         a_rows[at, mine] = rows_of(az_in, at)
-        tp_exchange(a_rows.at[at], a_rows.at[at], AR[at], False)
+        tp_exchange(a_rows.at[at], a_rows.at[at], AR[at], False, ROWS)
 
     bytes_of(asq_in, tp_count - 1, recv_sem.at[ASQ])
     squares = as_column(jnp.sum(asq_in[:, 0, :], axis=0, keepdims=True))
@@ -494,7 +496,7 @@
             ex_out[at, c] = jnp.dot(
                 active, downs[:, width * c : width * c + width], preferred_element_type=F32
             ).astype(BF16)
-        tp_exchange(ex_out.at[at], ex_in.at[at], EX[at], True)
+        tp_exchange(ex_out.at[at], ex_in.at[at], EX[at], True, OTHERS)
         ex_in[at, mine] = ex_out[at, mine]
 
     bytes_of(h_rows, tp_count - 1, recv_sem.at[HR])
@@ -514,7 +516,6 @@
         z_all(
             lambda to, off, other: back_out.at[2 * ((off + reach) % chips) + other],
             lambda off: back_in.at[me],
-            BACK,
             lambda off: BACK,
             [(rel - reach) % chips for rel in range(half * at, half * (at + 1))],
         )
@@ -527,31 +528,33 @@
             combined = combined + jnp.dot(mix_scr[s, part], table, preferred_element_type=F32)
 
     csq_in[mine] = as_row(combined)
-    tp_exchange(csq_in, csq_in, CSQ, False)
-
-    bytes_of(wq_all.at[:, 0], chips - 1, send_sem.at[WQ_SEND])
-    bytes_of(wq_all.at[:, 0], chips, send_sem.at[WQ_RELAY])
-    bytes_of(wo_all, chips - 1, send_sem.at[WO_SEND])
-    bytes_of(wo_all, chips, send_sem.at[WO_RELAY])
-    for ref, slot in ((hz_out, HZ), (az_out, AZ[0]), (back_out, BACK)):
-        bytes_of(ref, ep_count - 1, send_sem.at[slot])
-    for ref, slot in (
-        (rs_out, RS),
-        (h_rows, HR),
-        (asq_in, ASQ),
-        (a_rows.at[0], AR[0]),
-        (a_rows.at[1], AR[1]),
-        (ex_out.at[0], EX[0]),
-        (ex_out.at[1], EX[1]),
-    ):
-        bytes_of(ref, tp_count - 1, send_sem.at[slot])
+    tp_exchange(csq_in, csq_in, CSQ, False, OTHERS)
+
+    def size(ref, count):
+        total = count * ref.dtype.itemsize
+        for extent in ref.shape[1:]:
+            total *= extent
+        return total
+
+    def left(at, *parts):
+        row = gates.shape[1] * gates.dtype.itemsize
+        bytes_of(gates, sum(size(*part) for part in parts) // row, send_sem.at[at])
+
+    left(WEIGHTS, (wo_all, 2 * (2 * chips - 1)))
+    left(ROWS, (h_rows, tp_count - 1), (a_rows.at[0], 2 * (tp_count - 1)))
 
     bytes_of(csq_in, tp_count - 1, recv_sem.at[CSQ])
     squares = as_column(jnp.sum(csq_in[:, 0, :], axis=0, keepdims=True))
     out_gain = out_gain_ref[...].astype(F32).reshape(1, width)
     result = own_scr[...] + combined * inverse_rms(squares, features) * out_gain
     result_ref[...] = result.astype(BF16)
-    bytes_of(csq_in, tp_count - 1, send_sem.at[CSQ])
+    left(
+        OTHERS,
+        (rs_out, tp_count - 1),
+        (ex_out.at[0], 2 * (tp_count - 1)),
+        (asq_in, 2 * (tp_count - 1)),
+        (hz_out, 3 * (ep_count - 1)),
+    )
 
 
 def per_device(
@@ -608,7 +611,7 @@
         pltpu.VMEM((ep_count, 32, 128), BF16),
         pltpu.VMEM((64, features), BF16),
         pltpu.VMEM((16, positions), F32),
-        pltpu.VMEM((16, positions), BF16),
+        pltpu.VMEM((16, positions), F32),
         pltpu.VMEM((2, ep_count, sequences), BF16),
         pltpu.VMEM((2, 3, sequences, ep_count), BF16),
         pltpu.VMEM((sequences, width), F32),
@@ -630,12 +633,10 @@
         pltpu.VMEM((ep_count, 2, width), F32),
         pltpu.VMEM((tp_count, 1, width), F32),
         pltpu.VMEM((tp_count, 1, width), F32),
-        pltpu.SemaphoreType.DMA((5,)),
         pltpu.SemaphoreType.DMA((11,)),
-        pltpu.SemaphoreType.DMA((chips,)),
-        pltpu.SemaphoreType.DMA((chips,)),
-        pltpu.SemaphoreType.DMA((16,)),
-        pltpu.SemaphoreType.DMA((16,)),
+        pltpu.SemaphoreType.DMA((8,)),
+        pltpu.SemaphoreType.DMA((14,)),
+        pltpu.SemaphoreType.DMA((3,)),
     ]
     return pl.pallas_call(
         functools.partial(layer_kernel, ep_count, tp_count),

time: 64.2 us -> 63.2 us (0.984)
  Pallas kernels: 62.8 us -> 61.8 us
    pallas_call x1, Pallas kernels: 62.8 us -> 61.8 us  [per_device(): pl.pallas_call(functools.partial(layer_kernel, ep_count, tp_count), out_s...]
where the time goes in v4:
time: 63.2 us; the launch traced here: 63 us
  Pallas kernels  61.8 us (98%)
  between operations  0.66 us (1%)
    pallas_call x1, Pallas kernels, per_device(): pl.pallas_call(functools.partial(layer_kernel, ep_count, tp_count), out_s...  61.8 us

profile of v4, /device:TPU:1, one launch (start us, length us, event | category | flops | bytes accessed | tf_op | source)
XLA Modules:
  0.0 63.0 jit_solution(2806560545738706418)
XLA Ops:
  0.7 61.8 %layer.1 = bf16[12,128]{1,0:T(8,128)(2,1)S(1)} custom-call(bf16[12,2048]{1,0:T(8,128)(2,1)} %hidden_hbm.1, bf16[2048]{0:T(1024)(128)(2,1)} %pre_gain_hbm.1, bf16[64,64]{1,0:T(8,128)(2,1)} %query_weight_hbm.1, bf16[12,64,1024]{2,1,0:T(8,128)(2,1)} %key_hbm.1, bf16[12,64,1024]{2,1,0:T(8,128)(2,1)} %value_hbm.1, s32[12]{0:T(128)} %lengths_hbm.1, ...), custom_call_target="tpu_custom_call" | custom-call | tf_op jit(solution)/shard_map/layer/pallas_call | solution.py:641
  62.4 0.6 copy.18

commit v5 on v4

--- a/solution.py
+++ b/solution.py
@@ -78,7 +78,8 @@
     downs,
     wq_all,
     wo_all,
-    wo_full,
+    norm_scr,
+    side_scr,
     scores_scr,
     stick_scr,
     place_scr,
@@ -94,7 +95,6 @@
     az_in,
     h_rows,
     a_rows,
-    r_scr,
     f_scr,
     ex_out,
     ex_in,
@@ -134,16 +134,16 @@
     WQ_RELAY, WO_RELAY, HZ, HR, RS, ASQ, BACK, CSQ = range(8)
     AZ, AR, EX = (8, 9), (10, 11), (12, 13)
     WEIGHTS, ROWS, OTHERS = range(3)
-    line, spot = mine // side, lax.rem(mine, side)
+    line, column = mine // side, lax.rem(mine, side)
     steps = sorted(
         ((dy, dx) for dy in range(side) for dx in range(side) if dy + dx > 0),
         key=lambda step: -sum(min(d, side - d) for d in step),
     )
     others = [
-        lax.rem(line + dy, side) * side + lax.rem(spot + dx, side) for dy, dx in steps
+        lax.rem(line + dy, side) * side + lax.rem(column + dx, side) for dy, dx in steps
     ]
 
-    for off in range(1, reach + 1):
+    for off in range(reach, 0, -1):
         greet((2 * chip_at(off) + core, mine))
         greet((2 * chip_at(-off) + core, mine))
     greet((partner, mine))
@@ -184,9 +184,8 @@
         rows = value.shape[0] // 2
         return jnp.concatenate([value[:rows], value[rows:]], axis=1).astype(BF16)
 
-    wq_all[me, 0] = folded(query_weight_ref[...].astype(F32))
+    wq_all[me] = folded(query_weight_ref[...].astype(F32))
     wo_all[me] = folded(out_weight_ref[...].astype(F32))
-    wo_half = out_weight_ref.shape[0] // 2
 
     pl.semaphore_wait(barrier, 2 * reach + tp_count)
 
@@ -281,7 +280,7 @@
         some = ref.at[pl.ds(0, count)]
         pltpu.make_async_copy(some, some, sem).wait()
 
-    wq = weight(lambda owner: wq_all.at[owner, 0], 0, WQ_RELAY)
+    wq = weight(lambda owner: wq_all.at[owner], 0, WQ_RELAY)
     wo = weight(lambda owner: wo_all.at[owner], 4, WO_RELAY)
 
     send_near(wq)
@@ -299,6 +298,23 @@
         * pre_gain_ref[...].astype(F32).reshape(1, features)
     ).astype(BF16)
 
+    norm_scr[...] = jnp.zeros_like(norm_scr)
+    for c in range(chips):
+        norm_scr[c, 0:sequences, :] = normed[:, 128 * c : 128 * c + 128]
+    source, target = iota((128, 128), 0), iota((128, 128), 1)
+    piece, upper, spot = source // 64, lax.rem(source // 32, 2), lax.rem(source, 32)
+    turned = jnp.dot(
+        norm_scr[...].reshape(chips * 16, 128),
+        (target == upper * 64 + piece * 32 + spot).astype(BF16),
+        preferred_element_type=F32,
+    )
+    lower = iota((16, 128), 1) < 64
+    for c in range(0, chips, 2):
+        one, two = turned[16 * c : 16 * c + 16], turned[16 * c + 16 : 16 * c + 32]
+        columns = slice(64 * c, 64 * c + 128)
+        side_scr[0:16, columns] = jnp.where(lower, one, pltpu.roll(two, 64, 1)).astype(BF16)
+        side_scr[16:32, columns] = jnp.where(lower, pltpu.roll(one, 64, 1), two).astype(BF16)
+
     own_columns = pl.ds(pl.multiple_of(mine * width, width), width)
     own_scr[...] = hidden_ref[:, own_columns].astype(F32)
     scores_scr[...] = jnp.zeros_like(scores_scr)
@@ -317,16 +333,17 @@
     top = jnp.maximum(first, second)
     first, second = jnp.exp(first - top), jnp.exp(second - top)
     weighted = picks[0] * (first / (first + second)) + picks[1] * (second / (first + second))
-    for s in range(2):
-        at_slot = (earlier == float(s)).astype(F32)
-        place_scr[s] = (either * at_slot).astype(BF16)
-        for part, value in enumerate(three_parts(weighted * at_slot)):
-            mix_scr[s, part] = transposed(value).astype(BF16)
-
-    for s in range(2):
-        hz_out[:, s, :] = jnp.dot(
-            place_scr[s], own_scr[...].astype(BF16), preferred_element_type=F32
-        )
+    slots = [(earlier == float(s)).astype(F32) for s in range(2)]
+    place_scr[...] = jnp.concatenate([either * slot for slot in slots], axis=0).astype(BF16)
+    parts = [part.astype(F32) for slot in slots for part in three_parts(weighted * slot)]
+    mix_scr[...] = transposed(jnp.concatenate(parts, axis=0)).astype(BF16)
+
+    def place_rows(target, value):
+        placed = jnp.dot(place_scr[...], value, preferred_element_type=F32)
+        for s in range(2):
+            target[:, s, :] = placed[ep_count * s : ep_count * s + ep_count]
+
+    place_rows(hz_out, own_scr[...].astype(BF16))
 
     tri_scr[:, 0:128] = (iota((128, 128), 0) > iota((128, 128), 1)).astype(BF16)
     tri_scr[:, 128:256] = jnp.ones((128, 128), BF16)
@@ -338,20 +355,19 @@
 
     send_on(wq)
     send_on(wo)
-    bytes_of(wq_all.at[:, 0], inner, weight_sem.at[2])
+    bytes_of(wq_all, inner, weight_sem.at[2])
     hand_over(wq, near)
     bytes_of(wo_all, inner, weight_sem.at[6])
     hand_over(wo, near)
-    bytes_of(wq_all.at[:, 0], len(far), weight_sem.at[3])
+    bytes_of(wq_all, len(far), weight_sem.at[3])
     hand_over(wq, far)
-    bytes_of(wq_all.at[:, 0], chips, recv_sem.at[WQ_RELAY])
+    bytes_of(wq_all, chips, recv_sem.at[WQ_RELAY])
     spread(hz_out, hz_in, (HZ, HZ))
 
-    for i in range(ep_count):
-        wq_all[i, 1] = pltpu.roll(wq_all[i, 0].astype(F32), 64, 1).astype(BF16)
-    queries = jnp.dot(
-        normed, wq_all[...].reshape(features, 128), preferred_element_type=F32
-    )[:, 0:head_size]
+    product = jnp.dot(
+        side_scr[...], wq_all[...].reshape(features // 2, 128), preferred_element_type=F32
+    )
+    queries = (product[0:16] + pltpu.roll(product[16:32], 64, 1))[:, 0:head_size]
     query_columns = transposed(queries)
 
     bytes_of(wo_all, len(far), weight_sem.at[7])
@@ -396,21 +412,17 @@
         mixed_columns = jnp.where(
             column == b, jnp.sum(read, axis=1, keepdims=True), mixed_columns
         )
-    mixed = transposed(mixed_columns).astype(BF16)
+    folds = head_size // 2
+    mixed = jnp.concatenate(
+        [transposed(mixed_columns[:folds]), transposed(mixed_columns[folds:])], axis=0
+    ).astype(BF16)
 
     bytes_of(wo_all, chips, recv_sem.at[WO_RELAY])
-    left = iota((wo_half, 128), 1) < 64
     for c in range(chips):
-        one, two = wo_all[2 * c].astype(F32), wo_all[2 * c + 1].astype(F32)
-        columns = slice(128 * c, 128 * c + 128)
-        wo_full[0:wo_half, columns] = jnp.where(left, one, pltpu.roll(two, 64, 1)).astype(BF16)
-        wo_full[wo_half : 2 * wo_half, columns] = jnp.where(
-            left, pltpu.roll(one, 64, 1), two
-        ).astype(BF16)
-    for c in range(tp_count):
-        rs_out[c] = jnp.dot(
-            mixed, wo_full[:, width * c : width * c + width], preferred_element_type=F32
-        ).astype(BF16)
+        one = jnp.dot(mixed, wo_all[2 * c], preferred_element_type=F32)
+        two = jnp.dot(mixed, wo_all[2 * c + 1], preferred_element_type=F32)
+        swapped = pltpu.roll(jnp.where(lower, two[0:16], one[16:32]), 64, 1)
+        rs_out[c] = (jnp.where(lower, one[0:16], two[16:32]) + swapped).astype(BF16)
     tp_exchange(rs_out, rs_in, RS, True, OTHERS)
     rs_in[mine] = rs_out[mine]
 
@@ -420,10 +432,7 @@
         total = total + rs_in[c].astype(F32)
     attended = total[0:sequences].astype(BF16)
 
-    for s in range(2):
-        az_out[:, s, :] = jnp.dot(
-            place_scr[s], attended, preferred_element_type=F32
-        )
+    place_rows(az_out, attended)
     spread(az_out, az_in, AZ)
 
     diagonal = iota((sequences, 128), 0) == iota((sequences, 128), 1)
@@ -479,18 +488,13 @@
                 h_rows[c, at].astype(F32)
                 + a_rows[at, c].astype(F32) * scale * post_gain[:, columns]
             ).astype(BF16)
-            r_scr[at, c] = one
             one = one.astype(F32)
             square = square + one * one
+            f_scr[at, :, columns] = (one * ffn_gain[:, columns]).astype(BF16)
         scale = inverse_rms(jnp.sum(square, axis=1, keepdims=True), features)
-        for c in range(tp_count):
-            columns = slice(width * c, width * c + width)
-            f_scr[at, :, columns] = (
-                r_scr[at, c].astype(F32) * scale * ffn_gain[:, columns]
-            ).astype(BF16)
         ffn_in = f_scr[at]
-        gate_act = jnp.dot(ffn_in, gates[...], preferred_element_type=F32)
-        up_act = jnp.dot(ffn_in, ups[...], preferred_element_type=F32)
+        gate_act = jnp.dot(ffn_in, gates[...], preferred_element_type=F32) * scale
+        up_act = jnp.dot(ffn_in, ups[...], preferred_element_type=F32) * scale
         active = (gate_act / (1.0 + jnp.exp(-gate_act)) * up_act).astype(BF16)
         for c in range(tp_count):
             ex_out[at, c] = jnp.dot(
@@ -521,11 +525,10 @@
         )
     back_in[me] = back_out[2 * reach + core]
     bytes_of(back_in, ep_count - 1, recv_sem.at[BACK])
-    combined = jnp.zeros((sequences, width), F32)
-    for s in range(2):
-        table = back_in[:, s, :].astype(BF16)
-        for part in (2, 1, 0):
-            combined = combined + jnp.dot(mix_scr[s, part], table, preferred_element_type=F32)
+    tables = [back_in[:, s, :].astype(BF16) for s in range(2) for part in range(3)]
+    combined = jnp.dot(
+        mix_scr[...], jnp.concatenate(tables, axis=0), preferred_element_type=F32
+    )
 
     csq_in[mine] = as_row(combined)
     tp_exchange(csq_in, csq_in, CSQ, False, OTHERS)
@@ -607,13 +610,14 @@
         pltpu.VMEM(gate_experts.shape[1:], BF16),
         pltpu.VMEM(up_experts.shape[1:], BF16),
         pltpu.VMEM(down_experts.shape[1:], BF16),
-        pltpu.VMEM((ep_count, 2, 32, 128), BF16),
         pltpu.VMEM((ep_count, 32, 128), BF16),
-        pltpu.VMEM((64, features), BF16),
+        pltpu.VMEM((ep_count, 32, 128), BF16),
+        pltpu.VMEM((chips, 16, 128), BF16),
+        pltpu.VMEM((32, features // 2), BF16),
         pltpu.VMEM((16, positions), F32),
         pltpu.VMEM((16, positions), F32),
-        pltpu.VMEM((2, ep_count, sequences), BF16),
-        pltpu.VMEM((2, 3, sequences, ep_count), BF16),
+        pltpu.VMEM((2 * ep_count, sequences), BF16),
+        pltpu.VMEM((sequences, 6 * ep_count), BF16),
         pltpu.VMEM((sequences, width), F32),
         pltpu.VMEM((tp_count, 1, width), F32),
         pltpu.VMEM((128, 256), BF16),
@@ -624,7 +628,6 @@
         pltpu.VMEM((ep_count, 2, width), F32),
         pltpu.VMEM((ep_count, 2, width), F32),
         pltpu.VMEM((tp_count, 2, ep_count, width), BF16),
-        pltpu.VMEM((2, tp_count, ep_count, width), BF16),
         pltpu.VMEM((2, tp_count, ep_count, width), BF16),
         pltpu.VMEM((2, ep_count, features), BF16),
         pltpu.VMEM((2, tp_count, ep_count, width), BF16),

time: 63.2 us -> 63.1 us (level)
  no operation moved by 1% of the time
where the time goes in v5:
time: 63.1 us; the launch traced here: 63 us
  Pallas kernels  61.7 us (98%)
  between operations  0.66 us (1%)
    pallas_call x1, Pallas kernels, per_device(): pl.pallas_call(functools.partial(layer_kernel, ep_count, tp_count), out_s...  61.7 us

profile of v5, /device:TPU:1, one launch (start us, length us, event | category | flops | bytes accessed | tf_op | source)
XLA Modules:
  0.0 63.0 jit_solution(16113815345355635558)
XLA Ops:
  0.7 61.7 %layer.1 = bf16[12,128]{1,0:T(8,128)(2,1)S(1)} custom-call(bf16[12,2048]{1,0:T(8,128)(2,1)} %hidden_hbm.1, bf16[2048]{0:T(1024)(128)(2,1)} %pre_gain_hbm.1, bf16[64,64]{1,0:T(8,128)(2,1)} %query_weight_hbm.1, bf16[12,64,1024]{2,1,0:T(8,128)(2,1)} %key_hbm.1, bf16[12,64,1024]{2,1,0:T(8,128)(2,1)} %value_hbm.1, s32[12]{0:T(128)} %lengths_hbm.1, ...), custom_call_target="tpu_custom_call" | custom-call | tf_op jit(solution)/shard_map/layer/pallas_call | solution.py:644
  62.4 0.6 copy.18
